TPU v7x, 32 devices: a whole 2x2x4 slice. The times are simulated.
32 devices in a mesh: grp: 2 (over y), fs: 4 (over z), tp: 4 (over x, core).
Axes of the slice: x: 2, y: 2, z: 4, core: 2. Of those that a mesh axis runs over, the one named last changes fastest.
Arguments:
- prompt: bfloat16 [2048, 2048], P(('grp', 'tp')), parts along dimension 0, may hold values from -6 to 6
- gain_first: float32 [2048], P('fs'), may hold values from 0.1 to 1.9
- gate_first: float32 [2048, 4096], P('fs', 'tp'), may hold values from -0.125 to 0.125
- up_first: float32 [2048, 4096], P('fs', 'tp'), may hold values from -0.125 to 0.125
- down_first: float32 [4096, 2048], P('fs', 'tp'), may hold values from -0.09375 to 0.09375
- gain_second: float32 [2048], P('fs'), may hold values from 0.1 to 1.9
- gate_second: float32 [2048, 4096], P('fs', 'tp'), may hold values from -0.125 to 0.125
- up_second: float32 [2048, 4096], P('fs', 'tp'), may hold values from -0.125 to 0.125
- down_second: float32 [4096, 2048], P('fs', 'tp'), may hold values from -0.09375 to 0.09375
Outputs:
- result: bfloat16 [2048, 2048], P(('grp', 'tp')), parts along dimension 0
- served_gate_first: bfloat16 [4096, 4096], P('grp', 'fs'), parts along dimension 0
- served_up_first: bfloat16 [4096, 4096], P('grp', 'fs'), parts along dimension 0
- served_down_first: bfloat16 [4096, 4096], P('fs', 'grp'), parts along dimension 1
- served_gate_second: bfloat16 [4096, 4096], P('grp', 'fs'), parts along dimension 0
- served_up_second: bfloat16 [4096, 4096], P('grp', 'fs'), parts along dimension 0
- served_down_second: bfloat16 [4096, 4096], P('fs', 'grp'), parts along dimension 1
There are 2 independent parts, one for each index of `grp`. A program takes and returns all parts, laid end to end along the dimension named above; an argument that names none is the same for every part. Nothing has to cross between parts.
All inputs are finite; a program needn't handle non-finite values.
Results may differ from a plain program's by a relative error of at most 0.0053.
Values may be sent and summed in bfloat16 or wider, within the bound.
A program may use at most 128 MiB of HBM per device.

v0:
```python
import functools

import jax
import jax.numpy as jnp
from jax import lax
from jax.experimental import pallas as pl
from jax.experimental.pallas import tpu as pltpu
from jax.sharding import PartitionSpec as P

EPS = 1e-06
MESH = pl.DeviceIdType.MESH


def fold(gain, weight):
    return (gain[:, None] * weight).astype(jnp.bfloat16)


def kernel(n_grp, n_fs, n_tp, n_sub, *refs):
    prompt = refs[0]
    ins, in_down = refs[1:5], refs[5:7]
    out_result, outs, out_down = refs[7], refs[8:12], refs[12:14]
    served, served_down = refs[14:18], refs[18:20]
    stream, normed, hidden, part, landed, spread, stage = refs[20:27]
    (p_send, p_recv, r_send, z_send, z_recv, x_send, x_recv, y_send, y_recv, c_send, c_recv, own_sem,
     dx_send, dx_recv, dy_send, dy_recv, dc_send, dc_recv, down_own,
     rs_send, rs_recv, ag_send, ag_recv, out_sem) = refs[27:]

    g, f, t = lax.axis_index("grp"), lax.axis_index("fs"), lax.axis_index("tp")
    ratio = n_fs // n_tp
    chips = n_tp // 2
    home = f // ratio
    mine_sub = lax.rem(t + n_tp - home, n_tp) // 2
    carries = mine_sub < n_sub
    is_lane = lax.rem(t, 2) == lax.rem(home, 2)
    partner = t + 1 - 2 * lax.rem(t, 2)

    def along_fs(o):
        return lax.rem(f + o, n_fs)

    def along_tp(dx):
        return lax.rem(t + 2 * dx, n_tp)

    def along_grp(dg):
        return lax.rem(g + dg, n_grp)

    barrier = pltpu.get_barrier_semaphore()
    peers = (
        [{"fs": along_fs(o)} for o in range(1, n_fs)]
        + [{"tp": along_tp(dx)} for dx in range(1, chips)]
        + [{"grp": along_grp(dg)} for dg in range(1, n_grp)]
        + [{"tp": partner}]
    )
    for peer in peers:
        pl.semaphore_signal(barrier, inc=1, device_id=peer, device_id_type=MESH)
    pl.semaphore_wait(barrier, len(peers))

    def remote(src, dst, send, recv, where):
        return pltpu.make_async_remote_copy(
            src_ref=src, dst_ref=dst, send_sem=send, recv_sem=recv,
            device_id=where, device_id_type=MESH,
        )

    def arrived(dst, sem):
        pltpu.make_async_copy(dst, dst, sem).wait()

    rows = ins[0].shape[0]
    share = rows // n_grp
    sub = share // n_sub
    width = served[0].shape[1]
    d_rows = served_down[0].shape[0]
    d_share = d_rows // n_grp
    d_cols = in_down[0].shape[1]

    def piece(m, r, h, s):
        return served[m].at[pl.ds(pl.multiple_of(r * rows + h * share + s * sub, sub), sub)]

    def p_copy(m, s):
        src = ins[m].at[pl.ds(pl.multiple_of(g * share + s * sub, sub), sub)]
        return remote(src, stage.at[m, s - 1], p_send.at[m, s - 1], p_recv.at[m, s - 1], {"tp": along_tp(s)})

    def z_copy(m, s, j):
        columns = pl.ds(j * width, width)
        if s == 0:
            src = ins[m].at[pl.ds(pl.multiple_of(g * share, share), sub), columns]
            return src, piece(m, f, g, s), t * ratio + j
        source = lax.rem(t + n_tp - 2 * s, n_tp)
        return stage.at[m, s - 1, :, columns], piece(m, f, g, s), source * ratio + j

    def z_remote(m, s, j):
        src, dst, to = z_copy(m, s, j)
        send = z_send.at[m, j] if s == 0 else r_send.at[m, s - 1, j]
        return remote(src, dst, send, z_recv.at[m, f], {"fs": to})

    def z_start(m, s):
        for j in range(ratio):
            src, dst, to = z_copy(m, s, j)

            @pl.when(to != f)
            def _():
                z_remote(m, s, j).start()

            @pl.when(to == f)
            def _():
                pltpu.make_async_copy(src, dst, own_sem.at[m]).start()

    def relay(m):
        for s in range(1, n_sub):
            arrived(stage.at[m, s - 1], p_recv.at[m, s - 1])
            z_start(m, s)

    def x_copy(m, r, dx):
        ref = piece(m, r, g, mine_sub)
        return remote(ref, ref, x_send.at[m, r, dx - 1], x_recv.at[m, r, mine_sub], {"tp": along_tp(dx)})

    def y_copy(m, r, dg, s):
        ref = piece(m, r, g, s)
        return remote(ref, ref, y_send.at[m, r, dg - 1, s], y_recv.at[m, r, g, s], {"grp": along_grp(dg)})

    def c_copy(m, r, h, s):
        ref = piece(m, r, h, s)
        return remote(ref, ref, c_send.at[m, r, h, s], c_recv.at[m, r, h, s], {"tp": partner})

    def primary(m):
        @pl.when(is_lane)
        def _():
            @pl.loop(0, n_fs)
            def _(o):
                r = along_fs(o)

                @pl.when(carries)
                def _():
                    @pl.when(o == 0)
                    def _():
                        arrived(piece(m, r, g, mine_sub), own_sem.at[m])

                    @pl.when(o != 0)
                    def _():
                        arrived(piece(m, r, g, mine_sub), z_recv.at[m, r])

                    for dx in range(1, chips):
                        x_copy(m, r, dx).start()
                    for dg in range(1, n_grp):
                        y_copy(m, r, dg, mine_sub).start()
                    c_copy(m, r, g, mine_sub).start()

    def crossed(m):
        @pl.when(is_lane)
        def _():
            @pl.loop(0, n_fs)
            def _(o):
                r = along_fs(o)
                for s in range(n_sub):
                    @pl.when(mine_sub != s)
                    def _():
                        arrived(piece(m, r, g, s), x_recv.at[m, r, s])
                        for dg in range(1, n_grp):
                            y_copy(m, r, dg, s).start()
                        c_copy(m, r, g, s).start()

    def secondary(m):
        @pl.when(is_lane)
        def _():
            @pl.loop(0, n_fs)
            def _(o):
                r = along_fs(o)
                for dg in range(1, n_grp):
                    h = along_grp(dg)
                    for s in range(n_sub):
                        arrived(piece(m, r, h, s), y_recv.at[m, r, h, s])
                        c_copy(m, r, h, s).start()

        @pl.when(jnp.logical_not(is_lane))
        def _():
            @pl.loop(0, n_fs)
            def _(r):
                for h in range(n_grp):
                    for s in range(n_sub):
                        arrived(piece(m, r, h, s), c_recv.at[m, r, h, s])

        pltpu.make_async_copy(served[m], outs[m], out_sem.at[m]).start()

    def d_piece(k, s, h):
        return served_down[k].at[
            pl.ds(pl.multiple_of(h * d_share, d_share), d_share),
            pl.ds(pl.multiple_of(s * d_cols, d_cols), d_cols),
        ]

    def d_block(k, s):
        return served_down[k].at[:, pl.ds(pl.multiple_of(s * d_cols, d_cols), d_cols)]

    def dx_copy(k, dx):
        src = in_down[k].at[pl.ds(pl.multiple_of(g * d_share, d_share), d_share)]
        return remote(src, d_piece(k, t, g), dx_send.at[k, dx - 1], dx_recv.at[k, dx - 1], {"tp": along_tp(dx)})

    def dy_copy(k, dx, dg):
        ref = d_piece(k, lax.rem(t + n_tp - 2 * dx, n_tp), g)
        return remote(ref, ref, dy_send.at[k, dx - 1, dg - 1], dy_recv.at[k, dx - 1, dg - 1], {"grp": along_grp(dg)})

    def dc_own(k):
        return remote(in_down[k], d_block(k, t), dc_send.at[k, 0], dc_recv.at[k, 0], {"tp": partner})

    def dc_copy(k, dx):
        ref = d_block(k, lax.rem(t + n_tp - 2 * dx, n_tp))
        return remote(ref, ref, dc_send.at[k, dx], dc_recv.at[k, dx], {"tp": partner})

    def down_start(k):
        for dx in range(1, chips):
            dx_copy(k, dx).start()
        dc_own(k).start()
        pltpu.make_async_copy(in_down[k], d_block(k, t), down_own.at[k]).start()

    def down_primary(k):
        for dx in range(1, chips):
            source = lax.rem(t + n_tp - 2 * dx, n_tp)
            arrived(d_piece(k, source, g), dx_recv.at[k, dx - 1])
            for dg in range(1, n_grp):
                dy_copy(k, dx, dg).start()

    def down_secondary(k):
        for dx in range(1, chips):
            source = lax.rem(t + n_tp - 2 * dx, n_tp)
            for dg in range(1, n_grp):
                arrived(d_piece(k, source, lax.rem(g + n_grp - dg, n_grp)), dy_recv.at[k, dx - 1, dg - 1])
            dc_copy(k, dx).start()
        arrived(d_block(k, t), down_own.at[k])
        arrived(d_block(k, partner), dc_recv.at[k, 0])
        for dx in range(1, chips):
            arrived(d_block(k, lax.rem(partner + n_tp - 2 * dx, n_tp)), dc_recv.at[k, dx])
        pltpu.make_async_copy(served_down[k], out_down[k], out_sem.at[4 + k]).start()

    tokens, features = prompt.shape
    owned = tokens // n_fs
    slab = min(64, tokens)
    tile = min(256, width)
    wide = min(256, features)

    def rs_copy(k, o):
        to = along_fs(o)
        return remote(part.at[k, to], landed.at[k, f], rs_send.at[k, o - 1], rs_recv.at[k, f], {"fs": to})

    def ag_copy(k, o):
        return remote(spread.at[k, f], spread.at[k, f], ag_send.at[k, o - 1], ag_recv.at[k, f], {"fs": along_fs(o)})

    def multiply(k):
        w_gate, w_up, w_down = served[2 * k], served[2 * k + 1], served_down[k]

        @pl.loop(0, tokens // slab)
        def _(i):
            at = pl.ds(pl.multiple_of(i * slab, slab), slab)
            value = stream[at]
            scale = lax.rsqrt(jnp.mean(value * value, axis=-1, keepdims=True) + EPS)
            normed[at] = (value * scale).astype(jnp.bfloat16)

        @pl.loop(0, width // tile)
        def _(i):
            at = pl.ds(pl.multiple_of(i * tile, tile), tile)
            gate = jnp.dot(normed[...], w_gate[:, at], preferred_element_type=jnp.float32)
            up = jnp.dot(normed[...], w_up[:, at], preferred_element_type=jnp.float32)
            hidden[:, at] = (jax.nn.silu(gate) * up).astype(jnp.bfloat16)

    def project(k):
        w_down = served_down[k]

        @pl.loop(0, features // wide)
        def _(i):
            at = pl.ds(pl.multiple_of(i * wide, wide), wide)
            value = jnp.dot(hidden[...], w_down[:, at], preferred_element_type=jnp.float32)
            for to in range(n_fs):
                part[k, to, :, at] = value[to * owned : (to + 1) * owned].astype(jnp.bfloat16)

        for o in range(1, n_fs):
            rs_copy(k, o).start()

    def add_up(k, last):
        for o in range(1, n_fs):
            arrived(landed.at[k, along_fs(o)], rs_recv.at[k, along_fs(o)])
        mine = pl.ds(pl.multiple_of(f * owned, owned), owned)

        @pl.loop(0, features // wide)
        def _(i):
            at = pl.ds(pl.multiple_of(i * wide, wide), wide)
            total = part[k, f, :, at].astype(jnp.float32)
            for o in range(1, n_fs):
                total = total + landed[k, along_fs(o), :, at].astype(jnp.float32)
            total = 0.5 * total
            if last:
                total = stream[mine, at] + total
            spread[k, f, :, at] = total.astype(jnp.bfloat16)

        for o in range(1, n_fs):
            ag_copy(k, o).start()

    def collect(k):
        for o in range(1, n_fs):
            arrived(spread.at[k, along_fs(o)], ag_recv.at[k, along_fs(o)])

    for m in range(4):
        for s in range(1, n_sub):
            p_copy(m, s).start()
        z_start(m, 0)
        if m % 2 == 1:
            down_start(m // 2)

    stream[...] = prompt[...].astype(jnp.float32)

    relay(0)
    relay(1)
    primary(0)
    relay(2)
    primary(1)
    relay(3)
    crossed(0)
    primary(2)
    crossed(1)
    down_primary(0)
    primary(3)
    secondary(0)
    secondary(1)
    multiply(0)
    crossed(2)
    down_secondary(0)
    project(0)
    crossed(3)
    down_primary(1)
    secondary(2)
    add_up(0, False)
    secondary(3)
    collect(0)
    for to in range(n_fs):
        at = pl.ds(to * owned, owned)
        stream[at] = stream[at] + spread[0, to].astype(jnp.float32)
    multiply(1)
    down_secondary(1)
    project(1)
    add_up(1, True)
    collect(1)
    result_copy = pltpu.make_async_copy(spread.at[1], out_result, out_sem.at[6])
    result_copy.start()

    for m in range(4):
        for s in range(n_sub):
            if s > 0:
                p_copy(m, s).wait_send()
            for j in range(ratio):
                @pl.when(z_copy(m, s, j)[2] != f)
                def _():
                    z_remote(m, s, j).wait_send()

        @pl.when(is_lane)
        def _():
            @pl.loop(0, n_fs)
            def _(r):
                @pl.when(carries)
                def _():
                    for dx in range(1, chips):
                        x_copy(m, r, dx).wait_send()

                for s in range(n_sub):
                    for dg in range(1, n_grp):
                        y_copy(m, r, dg, s).wait_send()
                    for h in range(n_grp):
                        c_copy(m, r, h, s).wait_send()

        pltpu.make_async_copy(served[m], outs[m], out_sem.at[m]).wait()
    for k in range(2):
        dc_own(k).wait_send()
        for dx in range(1, chips):
            dx_copy(k, dx).wait_send()
            dc_copy(k, dx).wait_send()
            for dg in range(1, n_grp):
                dy_copy(k, dx, dg).wait_send()
        for o in range(1, n_fs):
            rs_copy(k, o).wait_send()
            ag_copy(k, o).wait_send()
        pltpu.make_async_copy(served_down[k], out_down[k], out_sem.at[4 + k]).wait()
    result_copy.wait()


def on_device(
    n_grp, n_fs, n_tp,
    prompt,
    gain_first,
    gate_first,
    up_first,
    down_first,
    gain_second,
    gate_second,
    up_second,
    down_second,
):
    own = (
        fold(gain_first, gate_first),
        fold(gain_first, up_first),
        fold(gain_second, gate_second),
        fold(gain_second, up_second),
        down_first.astype(jnp.bfloat16),
        down_second.astype(jnp.bfloat16),
    )
    tokens, features = prompt.shape
    width = gate_first.shape[1] * n_tp // n_fs
    d_rows = down_first.shape[0]
    owned = tokens // n_fs
    chips = n_tp // 2
    gate_shape, down_shape = (features, width), (d_rows, features)
    bf16 = functools.partial(jax.ShapeDtypeStruct, dtype=jnp.bfloat16)
    shapes = [(n_fs, owned, features)] + [gate_shape] * 4 + [down_shape] * 2
    share = gate_first.shape[0] // n_grp
    n_sub = chips if share % (16 * chips) == 0 else 1
    other_x, other_g = max(chips - 1, 1), max(n_grp - 1, 1)
    sems = [
        (4, other_x), (4, other_x), (4, other_x, n_fs // n_tp),
        (4, n_fs // n_tp), (4, n_fs), (4, n_fs, other_x), (4, n_fs, n_sub), (4, n_fs, other_g, n_sub),
        (4, n_fs, n_grp, n_sub), (4, n_fs, n_grp, n_sub), (4, n_fs, n_grp, n_sub), (4,),
        (2, other_x), (2, other_x), (2, other_x, other_g), (2, other_x, other_g),
        (2, chips), (2, chips), (2,),
        (2, n_fs), (2, n_fs), (2, n_fs), (2, n_fs), (7,),
    ]
    result, g1, u1, g2, u2, d1, d2 = pl.pallas_call(
        functools.partial(kernel, n_grp, n_fs, n_tp, n_sub),
        out_shape=[bf16(s) for s in shapes],
        in_specs=[pl.BlockSpec(memory_space=pltpu.VMEM)] + [pl.BlockSpec(memory_space=pl.ANY)] * 6,
        out_specs=[pl.BlockSpec(memory_space=pl.ANY)] * 7,
        scratch_shapes=[pltpu.VMEM(gate_shape, jnp.bfloat16)] * 4
        + [pltpu.VMEM(down_shape, jnp.bfloat16)] * 2
        + [
            pltpu.VMEM((tokens, features), jnp.float32),
            pltpu.VMEM((tokens, features), jnp.bfloat16),
            pltpu.VMEM((tokens, width), jnp.bfloat16),
            pltpu.VMEM((2, n_fs, owned, features), jnp.bfloat16),
            pltpu.VMEM((2, n_fs, owned, features), jnp.bfloat16),
            pltpu.VMEM((2, n_fs, owned, features), jnp.bfloat16),
            pltpu.VMEM((4, other_x, share // n_sub, gate_first.shape[1]), jnp.bfloat16),
        ]
        + [pltpu.SemaphoreType.DMA(s) for s in sems],
        compiler_params=pltpu.CompilerParams(
            collective_id=0, has_side_effects=True, vmem_limit_bytes=56 * 2**20
        ),
        name="serve",
    )(prompt, *own)
    return (result.reshape(tokens, features), g1, u1, d1, g2, u2, d2)


def solution(mesh):
    return jax.shard_map(
        functools.partial(on_device, mesh.shape["grp"], mesh.shape["fs"], mesh.shape["tp"]),
        mesh=mesh,
        in_specs=(
            P(("grp", "tp"), None),
            P("fs"),
            P("fs", "tp"),
            P("fs", "tp"),
            P("fs", "tp"),
            P("fs"),
            P("fs", "tp"),
            P("fs", "tp"),
            P("fs", "tp"),
        ),
        out_specs=(
            P(("grp", "tp"), None),
            P("grp", "fs"),
            P("grp", "fs"),
            P("fs", "grp"),
            P("grp", "fs"),
            P("grp", "fs"),
            P("fs", "grp"),
        ),
        check_vma=False,
    )
```

profile of v0, /device:TPU:16, one launch (start us, length us, event | category | flops | bytes accessed | tf_op | source)
XLA Modules:
  0.0 253.2 jit_solution(10704216505199870883)
XLA Ops:
  0.6 0.0 copy-start.5
  0.6 0.0 copy-start.7
  0.7 2.8 %convert_element_type.22.refs_5_ = bf16[1024,512]{1,0:T(8,128)(2,1)} convert(f32[1024,512]{1,0:T(8,128)} %param.13) | non-fusion elementwise | flops 524288 | bytes 3145728 | tf_op jit(solution)/shard_map/convert_element_type | solution.py:396
  3.5 0.0 copy-done.5
  3.5 0.0 copy-start.6
  3.5 1.1 convert_element_type.23.refs_6_
  4.6 0.0 copy-done.7
  4.6 0.9 copy-done.6
  5.5 4.7 %multiply_convert_fusion = (bf16[512,1024]{1,0:T(8,128)(2,1)}, bf16[512,1024]{1,0:T(8,128)(2,1)}, bf16[512,1024]{1,0:T(8,128)(2,1)}, bf16[512,1024]{1,0:T(8,128)(2,1)}) fusion(f32[512,1024]{1,0:T(8,128)S(1)} %copy-done.6, f32[512]{0:T(512)} %param.14, f32[512,1024]{1,0:T(8,128)S(1)} %copy-done.7, f32[512,1024]{1,0:T(8,128)} %param.11, f32[512]{0:T(512)} %param.10, ...), kind=kLoop, calls=%fused_computation | loop fusion | flops 4194304 | bytes 12587008 | tf_op jit(solution)/shard_map/convert_element_type | solution.py:15
  10.2 219.1 %serve.1 = (bf16[4,64,2048]{2,1,0:T(8,128)(2,1)}, bf16[2048,1024]{1,0:T(8,128)(2,1)}, bf16[2048,1024]{1,0:T(8,128)(2,1)}, bf16[2048,1024]{1,0:T(8,128)(2,1)}, bf...) custom-call(bf16[256,2048]{1,0:T(8,128)(2,1)} %refs_0_.1, ...), custom_call_target="tpu_custom_call" | custom-call | tf_op jit(solution)/shard_map/serve/pallas_call | solution.py:418
  229.3 2.3 copy.23
  231.6 0.0 copy-start.4
  231.6 4.8 %copy.24 = bf16[2048,1024]{1,0:T(8,128)(2,1)} copy(bf16[2048,1024]{1,0:T(8,128)(2,1)} %get-tuple-element.35) | data formatting | bytes 8388608
  236.4 0.0 copy-done.4
  236.4 0.0 copy-start.3
  236.4 2.1 copy.25
  238.5 1.6 copy-done.3
  240.1 0.0 copy-start.2
  240.1 2.1 copy.26
  242.2 1.6 copy-done.2
  243.8 0.0 copy-start.1
  243.8 2.1 copy.27
  245.9 1.6 copy-done.1
  247.5 0.0 copy-start
  247.5 2.1 copy.28
  249.6 1.6 copy-done
  251.2 2.0 copy.29
Async XLA Ops:
  0.6 2.9 %copy-start.5 = (f32[1024,512]{1,0:T(8,128)S(1)}, f32[1024,512]{1,0:T(8,128)}, u32[]{:S(2)}) copy-start(f32[1024,512]{1,0:T(8,128)} %param.17) | copy-start | bytes 6291460
  0.6 4.0 %copy-start.7 = (f32[512,1024]{1,0:T(8,128)S(1)}, f32[512,1024]{1,0:T(8,128)}, u32[]{:S(2)}) copy-start(f32[512,1024]{1,0:T(8,128)} %param.15) | copy-start | bytes 6291460
  3.5 2.0 copy-start.6
  231.6 4.8 %copy-start.4 = (bf16[2048,1024]{1,0:T(8,128)(2,1)S(1)}, bf16[2048,1024]{1,0:T(8,128)(2,1)}, u32[]{:S(2)}) copy-start(bf16[2048,1024]{1,0:T(8,128)(2,1)} %get-tuple-element.36) | copy-start | bytes 12582916
  236.4 3.7 %copy-start.3 = (bf16[1024,2048]{1,0:T(8,128)(2,1)S(1)}, bf16[1024,2048]{1,0:T(8,128)(2,1)}, u32[]{:S(2)}) copy-start(bf16[1024,2048]{1,0:T(8,128)(2,1)} %get-tuple-element.37) | copy-start | bytes 12582916
  240.1 3.7 %copy-start.2 = (bf16[2048,1024]{1,0:T(8,128)(2,1)S(1)}, bf16[2048,1024]{1,0:T(8,128)(2,1)}, u32[]{:S(2)}) copy-start(bf16[2048,1024]{1,0:T(8,128)(2,1)} %get-tuple-element.38) | copy-start | bytes 12582916
  243.8 3.7 %copy-start.1 = (bf16[2048,1024]{1,0:T(8,128)(2,1)S(1)}, bf16[2048,1024]{1,0:T(8,128)(2,1)}, u32[]{:S(2)}) copy-start(bf16[2048,1024]{1,0:T(8,128)(2,1)} %get-tuple-element.39) | copy-start | bytes 12582916
  247.5 3.7 %copy-start = (bf16[1024,2048]{1,0:T(8,128)(2,1)S(1)}, bf16[1024,2048]{1,0:T(8,128)(2,1)}, u32[]{:S(2)}) copy-start(bf16[1024,2048]{1,0:T(8,128)(2,1)} %get-tuple-element.40) | copy-start | bytes 12582916
where the time goes:
time: 254 us; the launch traced here: 253 us
  Pallas kernels  219 us (86%)
  local copies, waits for them, and re-layouts  24.8 us (10%)
  other arithmetic  8.68 us (3%)
    pallas_call x1, Pallas kernels, on_device(): pl.pallas_call(functools.partial(kernel, n_grp, n_fs, n_tp, n_sub), out_s...  219 us
    unnamed x23, local copies, waits for them, and re-layouts  24.8 us

commit v1 on v0

v1 whole, which is shorter than its diff:
```python
import functools

import jax
import jax.numpy as jnp
from jax import lax
from jax.experimental import pallas as pl
from jax.experimental.pallas import tpu as pltpu
from jax.sharding import PartitionSpec as P

EPS = 1e-06
MESH = pl.DeviceIdType.MESH
LANES = 128
LAG = 2


def kernel(n_grp, n_fs, n_tp, n_sub, *refs):
    prompt, gains, weights, downs = refs[0], refs[1:3], refs[3:7], refs[7:9]
    result, served, served_down = refs[9], refs[10:14], refs[14:16]
    (land, own, scale, stream, normed, hidden, onward, inward, middle, delta, stage) = refs[16:27]
    (load_sem, prompt_sem,
     p_send, p_recv, r_send, z_send, z_recv, x_send, x_recv, y_send, y_recv, c_send, c_recv, own_sem,
     dx_send, dx_recv, dy_send, dy_recv, dc_send, dc_recv,
     s_send, u_recv, m_recv, o_send, o_recv) = refs[27:]

    g, f, t = lax.axis_index("grp"), lax.axis_index("fs"), lax.axis_index("tp")
    ratio = n_fs // n_tp
    chips = n_tp // 2
    home = f // ratio
    mine_sub = lax.rem(t + n_tp - home, n_tp) // 2
    carries = mine_sub < n_sub
    is_lane = lax.rem(t, 2) == lax.rem(home, 2)
    partner = t + 1 - 2 * lax.rem(t, 2)

    half = n_fs // 2
    lower = f < half
    is_mid = jnp.logical_or(f == half - 1, f == half)
    is_end = jnp.logical_or(f == 0, f == n_fs - 1)
    toward = jnp.where(lower, f + 1, f - 1)
    away = jnp.where(lower, jnp.maximum(f - 1, 0), jnp.minimum(f + 1, n_fs - 1))

    def along_fs(o):
        return lax.rem(f + o, n_fs)

    def along_tp(dx):
        return lax.rem(t + 2 * dx, n_tp)

    def along_grp(dg):
        return lax.rem(g + dg, n_grp)

    def remote(src, dst, send, recv, where):
        return pltpu.make_async_remote_copy(
            src_ref=src, dst_ref=dst, send_sem=send, recv_sem=recv,
            device_id=where, device_id_type=MESH,
        )

    def arrived(dst, sem):
        pltpu.make_async_copy(dst, dst, sem).wait()

    rows, columns = weights[0].shape
    share = rows // n_grp
    sub = share // n_sub
    width = served[0].shape[1]
    d_rows, d_cols = downs[0].shape
    d_share = d_rows // n_grp
    tokens, features = prompt.shape
    slab = min(64, tokens)
    tile = min(256, width)
    wide = min(256, features)
    chunks = features // wide

    def landing(n):
        return land[n % 3] if n < 4 else land[3]

    def load(n):
        src = weights[n] if n < 4 else downs[n - 4]
        return pltpu.make_async_copy(src, landing(n), load_sem.at[n])

    def spread_gain(k):
        gain = gains[k]
        if gain.shape[0] == rows:
            scale[k] = gain[...]
        else:
            scale[k] = jnp.broadcast_to(gain[...], (LANES, rows)).T

    def fold(m):
        load(m).wait()
        step = min(64, rows)

        @pl.loop(0, rows // step)
        def _(i):
            at = pl.ds(pl.multiple_of(i * step, step), step)
            factor = scale[m // 2, at]
            for j in range(columns // LANES):
                lanes = pl.ds(j * LANES, LANES)
                own[m, at, lanes] = (factor * landing(m)[at, lanes]).astype(jnp.bfloat16)

    def round_down(k):
        load(4 + k).wait()
        step = min(64, d_rows)

        @pl.loop(0, d_rows // step)
        def _(i):
            at = pl.ds(pl.multiple_of(i * step, step), step)
            to = pl.ds(pl.multiple_of(t * d_cols, d_cols), d_cols)
            served_down[k][at, to] = landing(4 + k)[at].astype(jnp.bfloat16)

    def piece(m, r, h, s):
        return served[m].at[pl.ds(pl.multiple_of(r * rows + h * share + s * sub, sub), sub)]

    def p_copy(m, s):
        src = own.at[m, pl.ds(pl.multiple_of(g * share + s * sub, sub), sub)]
        return remote(src, stage.at[m, s - 1], p_send.at[m, s - 1], p_recv.at[m, s - 1], {"tp": along_tp(s)})

    def p_start(m):
        for s in range(1, n_sub):
            p_copy(m, s).start()

    def z_copy(m, s, j):
        cut = pl.ds(j * width, width)
        if s == 0:
            src = own.at[m, pl.ds(pl.multiple_of(g * share, share), sub), cut]
            return src, piece(m, f, g, s), t * ratio + j
        source = lax.rem(t + n_tp - 2 * s, n_tp)
        return stage.at[m, s - 1, :, cut], piece(m, f, g, s), source * ratio + j

    def z_remote(m, s, j):
        src, dst, to = z_copy(m, s, j)
        send = z_send.at[m, j] if s == 0 else r_send.at[m, s - 1, j]
        return remote(src, dst, send, z_recv.at[m, f], {"fs": to})

    def z_start(m, s):
        for j in range(ratio):
            src, dst, to = z_copy(m, s, j)

            @pl.when(to != f)
            def _():
                z_remote(m, s, j).start()

            @pl.when(to == f)
            def _():
                pltpu.make_async_copy(src, dst, own_sem.at[m]).start()

    def relay(m):
        for s in range(1, n_sub):
            arrived(stage.at[m, s - 1], p_recv.at[m, s - 1])
            z_start(m, s)

    def x_copy(m, r, dx):
        ref = piece(m, r, g, mine_sub)
        return remote(ref, ref, x_send.at[m, r, dx - 1], x_recv.at[m, r, mine_sub], {"tp": along_tp(dx)})

    def y_copy(m, r, dg, s):
        ref = piece(m, r, g, s)
        return remote(ref, ref, y_send.at[m, r, dg - 1, s], y_recv.at[m, r, g, s], {"grp": along_grp(dg)})

    def c_copy(m, r, h, s):
        ref = piece(m, r, h, s)
        return remote(ref, ref, c_send.at[m, r, h, s], c_recv.at[m, r, h, s], {"tp": partner})

    def primary(m):
        @pl.when(is_lane)
        def _():
            @pl.loop(0, n_fs)
            def _(o):
                r = along_fs(o)

                @pl.when(carries)
                def _():
                    @pl.when(o == 0)
                    def _():
                        arrived(piece(m, r, g, mine_sub), own_sem.at[m])

                    @pl.when(o != 0)
                    def _():
                        arrived(piece(m, r, g, mine_sub), z_recv.at[m, r])

                    for dx in range(1, chips):
                        x_copy(m, r, dx).start()
                    for dg in range(1, n_grp):
                        y_copy(m, r, dg, mine_sub).start()
                    c_copy(m, r, g, mine_sub).start()

    def crossed_step(m, o):
        r = along_fs(o)
        for s in range(n_sub):
            @pl.when(mine_sub != s)
            def _():
                arrived(piece(m, r, g, s), x_recv.at[m, r, s])
                for dg in range(1, n_grp):
                    y_copy(m, r, dg, s).start()
                c_copy(m, r, g, s).start()

    def crossed(m):
        @pl.when(is_lane)
        def _():
            @pl.loop(0, n_fs)
            def _(o):
                crossed_step(m, o)

    def secondary(m):
        @pl.when(is_lane)
        def _():
            @pl.loop(0, n_fs)
            def _(o):
                r = along_fs(o)
                for dg in range(1, n_grp):
                    h = along_grp(dg)
                    for s in range(n_sub):
                        arrived(piece(m, r, h, s), y_recv.at[m, r, h, s])
                        c_copy(m, r, h, s).start()

    def complete(m):
        @pl.when(jnp.logical_not(is_lane))
        def _():
            @pl.loop(0, n_fs)
            def _(r):
                for h in range(n_grp):
                    for s in range(n_sub):
                        arrived(piece(m, r, h, s), c_recv.at[m, r, h, s])

    direct = (True, False)

    def d_piece(k, s, h):
        return served_down[k].at[
            pl.ds(pl.multiple_of(h * d_share, d_share), d_share),
            pl.ds(pl.multiple_of(s * d_cols, d_cols), d_cols),
        ]

    def d_block(k, s):
        return served_down[k].at[:, pl.ds(pl.multiple_of(s * d_cols, d_cols), d_cols)]

    def d_first(k, s):
        return d_block(k, s) if direct[k] else d_piece(k, s, g)

    def dx_copy(k, dx):
        ref = d_first(k, t)
        return remote(ref, ref, dx_send.at[k, dx - 1], dx_recv.at[k, dx - 1], {"tp": along_tp(dx)})

    def dy_copy(k, dx, dg):
        ref = d_piece(k, lax.rem(t + n_tp - 2 * dx, n_tp), g)
        return remote(ref, ref, dy_send.at[k, dx - 1, dg - 1], dy_recv.at[k, dx - 1, dg - 1], {"grp": along_grp(dg)})

    def dc_copy(k, dx):
        ref = d_block(k, lax.rem(t + n_tp - 2 * dx, n_tp))
        return remote(ref, ref, dc_send.at[k, dx], dc_recv.at[k, dx], {"tp": partner})

    def down_start(k):
        for dx in range(1, chips):
            dx_copy(k, dx).start()
        dc_copy(k, 0).start()

    def down_primary(k):
        if direct[k]:
            return
        for dx in range(1, chips):
            source = lax.rem(t + n_tp - 2 * dx, n_tp)
            arrived(d_piece(k, source, g), dx_recv.at[k, dx - 1])
            for dg in range(1, n_grp):
                dy_copy(k, dx, dg).start()

    def down_secondary(k):
        for dx in range(1, chips):
            source = lax.rem(t + n_tp - 2 * dx, n_tp)
            if direct[k]:
                arrived(d_block(k, source), dx_recv.at[k, dx - 1])
            else:
                for dg in range(1, n_grp):
                    arrived(d_piece(k, source, lax.rem(g + n_grp - dg, n_grp)), dy_recv.at[k, dx - 1, dg - 1])
            dc_copy(k, dx).start()
        for dx in range(chips):
            arrived(d_block(k, lax.rem(partner + n_tp - 2 * dx, n_tp)), dc_recv.at[k, dx])

    final = (delta, result)

    def to_middle(k, i):
        return remote(onward.at[k, i], middle.at[k, i], s_send.at[k, i], m_recv.at[k, i], {"fs": toward})

    def to_next(k, i):
        return remote(onward.at[k, i], inward.at[k, i], s_send.at[k, i], u_recv.at[k, i], {"fs": toward})

    def to_outer(k, i):
        ref = final[k].at[i]
        return remote(ref, ref, o_send.at[k, i], o_recv.at[k, i], {"fs": away})

    def gather_in(k, i):
        at = pl.ds(pl.multiple_of(i * wide, wide), wide)
        value = jnp.dot(hidden[...], served_down[k][:, at], preferred_element_type=jnp.float32)

        @pl.when(is_end)
        def _():
            onward[k, i] = value.astype(jnp.bfloat16)

        @pl.when(jnp.logical_not(is_end))
        def _():
            arrived(inward.at[k, i], u_recv.at[k, i])
            onward[k, i] = (value + inward[k, i].astype(jnp.float32)).astype(jnp.bfloat16)

        @pl.when(is_mid)
        def _():
            to_middle(k, i).start()

        @pl.when(jnp.logical_not(is_mid))
        def _():
            to_next(k, i).start()

    def spread_out(k, i):
        at = pl.ds(pl.multiple_of(i * wide, wide), wide)

        @pl.when(is_mid)
        def _():
            arrived(middle.at[k, i], m_recv.at[k, i])
            total = 0.5 * (onward[k, i].astype(jnp.float32) + middle[k, i].astype(jnp.float32))
            if k == 1:
                total = stream[:, at] + total
            final[k][i] = total.astype(jnp.bfloat16)

        @pl.when(jnp.logical_not(is_mid))
        def _():
            arrived(final[k].at[i], o_recv.at[k, i])

        @pl.when(jnp.logical_not(is_end))
        def _():
            to_outer(k, i).start()

        if k == 0:
            stream[:, at] = stream[:, at] + delta[i].astype(jnp.float32)

    def reduce(k, beside=None):
        @pl.loop(0, chunks + LAG)
        def _(i):
            @pl.when(i < chunks)
            def _():
                gather_in(k, i)
                if beside is not None:
                    beside(i)

            @pl.when(i >= LAG)
            def _():
                spread_out(k, i - LAG)

    def norm():
        @pl.loop(0, tokens // slab)
        def _(i):
            at = pl.ds(pl.multiple_of(i * slab, slab), slab)
            value = stream[at]
            factor = lax.rsqrt(jnp.mean(value * value, axis=-1, keepdims=True) + EPS)
            normed[at] = (value * factor).astype(jnp.bfloat16)

    def multiply(k):
        w_gate, w_up = served[2 * k], served[2 * k + 1]

        @pl.loop(0, width // tile)
        def _(i):
            at = pl.ds(pl.multiple_of(i * tile, tile), tile)
            gate = jnp.dot(normed[...], w_gate[:, at], preferred_element_type=jnp.float32)
            up = jnp.dot(normed[...], w_up[:, at], preferred_element_type=jnp.float32)
            hidden[:, at] = (jax.nn.silu(gate) * up).astype(jnp.bfloat16)

    for n in (0, 1, 2, 4):
        load(n).start()
    prompt_copy = pltpu.make_async_copy(prompt, normed, prompt_sem)
    prompt_copy.start()

    barrier = pltpu.get_barrier_semaphore()
    peers = (
        [{"fs": along_fs(o)} for o in range(1, n_fs)]
        + [{"tp": along_tp(dx)} for dx in range(1, chips)]
        + [{"grp": along_grp(dg)} for dg in range(1, n_grp)]
        + [{"tp": partner}]
    )
    for peer in peers:
        pl.semaphore_signal(barrier, inc=1, device_id=peer, device_id_type=MESH)
    spread_gain(0)
    fold(0)
    pl.semaphore_wait(barrier, len(peers))

    p_start(0)
    z_start(0, 0)
    load(3).start()
    fold(1)
    p_start(1)
    z_start(1, 0)
    spread_gain(1)
    round_down(0)
    load(5).start()
    fold(2)
    fold(3)
    round_down(1)
    prompt_copy.wait()
    stream[...] = normed[...].astype(jnp.float32)
    norm()

    relay(0)
    relay(1)
    primary(0)
    p_start(2)
    z_start(2, 0)
    primary(1)
    p_start(3)
    z_start(3, 0)
    crossed(0)
    relay(2)
    down_start(0)
    crossed(1)
    relay(3)
    primary(2)
    primary(3)
    down_secondary(0)
    secondary(0)
    secondary(1)
    complete(0)
    complete(1)
    multiply(0)
    down_start(1)

    def beside(i):
        @pl.when(is_lane)
        def _():
            per = -(-2 * n_fs // chunks)
            for q in range(per):
                n = i * per + q

                @pl.when(n < n_fs)
                def _():
                    crossed_step(2, n)

                @pl.when(jnp.logical_and(n >= n_fs, n < 2 * n_fs))
                def _():
                    crossed_step(3, n - n_fs)

    reduce(0, beside)
    norm()
    down_primary(1)
    secondary(2)
    secondary(3)
    complete(2)
    complete(3)
    multiply(1)
    down_secondary(1)
    reduce(1)

    for m in range(4):
        for s in range(n_sub):
            if s > 0:
                p_copy(m, s).wait_send()
            for j in range(ratio):
                @pl.when(z_copy(m, s, j)[2] != f)
                def _():
                    z_remote(m, s, j).wait_send()

        @pl.when(is_lane)
        def _():
            @pl.loop(0, n_fs)
            def _(r):
                @pl.when(carries)
                def _():
                    for dx in range(1, chips):
                        x_copy(m, r, dx).wait_send()

                for s in range(n_sub):
                    for dg in range(1, n_grp):
                        y_copy(m, r, dg, s).wait_send()
                    for h in range(n_grp):
                        c_copy(m, r, h, s).wait_send()

    for k in range(2):
        dc_copy(k, 0).wait_send()
        for dx in range(1, chips):
            dx_copy(k, dx).wait_send()
            dc_copy(k, dx).wait_send()
            if not direct[k]:
                for dg in range(1, n_grp):
                    dy_copy(k, dx, dg).wait_send()

        @pl.loop(0, chunks)
        def _(i):
            @pl.when(is_mid)
            def _():
                to_middle(k, i).wait_send()

            @pl.when(jnp.logical_not(is_mid))
            def _():
                to_next(k, i).wait_send()

            @pl.when(jnp.logical_not(is_end))
            def _():
                to_outer(k, i).wait_send()


def store(parts, *refs):
    ins, outs, sems = refs[:7], refs[7:14], refs[14]
    copies = []
    chunks, _, wide = ins[0].shape
    for i in range(chunks):
        copies.append((ins[0].at[i], outs[0].at[:, pl.ds(i * wide, wide)]))
    for src, dst in zip(ins[1:], outs[1:]):
        rows = src.shape[0] // parts
        for i in range(parts):
            at = pl.ds(i * rows, rows)
            copies.append((src.at[at], dst.at[at]))
    copies = [pltpu.make_async_copy(src, dst, sems.at[i]) for i, (src, dst) in enumerate(copies)]
    for copy in copies:
        copy.start()
    for copy in copies:
        copy.wait()


def on_device(
    n_grp, n_fs, n_tp,
    prompt,
    gain_first,
    gate_first,
    up_first,
    down_first,
    gain_second,
    gate_second,
    up_second,
    down_second,
):
    tokens, features = prompt.shape
    rows, columns = gate_first.shape
    width = columns * n_tp // n_fs
    d_rows, d_cols = down_first.shape
    chips = n_tp // 2
    wide = min(256, features)
    chunks = features // wide
    gate_shape, down_shape = (features, width), (d_rows, features)
    bf16 = functools.partial(jax.ShapeDtypeStruct, dtype=jnp.bfloat16)
    share = rows // n_grp
    n_sub = chips if share % (16 * chips) == 0 else 1
    other_x, other_g = max(chips - 1, 1), max(n_grp - 1, 1)
    sems = [
        (6,), (),
        (4, other_x), (4, other_x), (4, other_x, n_fs // n_tp),
        (4, n_fs // n_tp), (4, n_fs), (4, n_fs, other_x), (4, n_fs, n_sub), (4, n_fs, other_g, n_sub),
        (4, n_fs, n_grp, n_sub), (4, n_fs, n_grp, n_sub), (4, n_fs, n_grp, n_sub), (4,),
        (2, other_x), (2, other_x), (2, other_x, other_g), (2, other_x, other_g),
        (2, chips), (2, chips),
        (2, chunks), (2, chunks), (2, chunks), (2, chunks), (2, chunks),
    ]
    if rows % LANES == 0:
        gains = [gain.reshape(1, rows) for gain in (gain_first, gain_second)]
    else:
        gains = [jnp.broadcast_to(gain[:, None], (rows, LANES)) for gain in (gain_first, gain_second)]
    far = functools.partial(pltpu.with_memory_space_constraint, memory_space=pltpu.HBM)
    vmem, hbm = pl.BlockSpec(memory_space=pltpu.VMEM), pl.BlockSpec(memory_space=pltpu.HBM)
    shapes = [(chunks, tokens, wide)] + [gate_shape] * 4 + [down_shape] * 2
    held = pl.pallas_call(
        functools.partial(kernel, n_grp, n_fs, n_tp, n_sub),
        out_shape=[bf16(s) for s in shapes],
        in_specs=[hbm] + [vmem] * 2 + [hbm] * 6,
        out_specs=[vmem] * 7,
        scratch_shapes=[
            [pltpu.VMEM((rows, columns), jnp.float32)] * 3 + [pltpu.VMEM((d_rows, d_cols), jnp.float32)],
            pltpu.VMEM((4, rows, columns), jnp.bfloat16),
            pltpu.VMEM((2, rows, LANES), jnp.float32),
            pltpu.VMEM((tokens, features), jnp.float32),
            pltpu.VMEM((tokens, features), jnp.bfloat16),
            pltpu.VMEM((tokens, width), jnp.bfloat16),
            pltpu.VMEM((2, chunks, tokens, wide), jnp.bfloat16),
            pltpu.VMEM((2, chunks, tokens, wide), jnp.bfloat16),
            pltpu.VMEM((2, chunks, tokens, wide), jnp.bfloat16),
            pltpu.VMEM((chunks, tokens, wide), jnp.bfloat16),
            pltpu.VMEM((4, other_x, share // n_sub, columns), jnp.bfloat16),
        ]
        + [pltpu.SemaphoreType.DMA(s) for s in sems],
        compiler_params=pltpu.CompilerParams(
            collective_id=0, has_side_effects=True, vmem_limit_bytes=26 * 2**20
        ),
        name="serve",
    )(far(prompt), *gains, *map(far, (gate_first, up_first, gate_second, up_second, down_first, down_second)))
    parts = 4
    result, g1, u1, g2, u2, d1, d2 = pl.pallas_call(
        functools.partial(store, parts),
        out_shape=[bf16((tokens, features))] + [bf16(s) for s in shapes[1:]],
        in_specs=[vmem] * 7,
        out_specs=[hbm] * 7,
        scratch_shapes=[pltpu.SemaphoreType.DMA((chunks + 6 * parts,))],
        compiler_params=pltpu.CompilerParams(vmem_limit_bytes=2**20),
        name="store",
    )(*held)
    return (result, g1, u1, d1, g2, u2, d2)
def solution(mesh):
    return jax.shard_map(
        functools.partial(on_device, mesh.shape["grp"], mesh.shape["fs"], mesh.shape["tp"]),
        mesh=mesh,
        in_specs=(
            P(("grp", "tp"), None),
            P("fs"),
            P("fs", "tp"),
            P("fs", "tp"),
            P("fs", "tp"),
            P("fs"),
            P("fs", "tp"),
            P("fs", "tp"),
            P("fs", "tp"),
        ),
        out_specs=(
            P(("grp", "tp"), None),
            P("grp", "fs"),
            P("grp", "fs"),
            P("fs", "grp"),
            P("grp", "fs"),
            P("grp", "fs"),
            P("fs", "grp"),
        ),
        check_vma=False,
    )
```

time: 254 us -> 239 us (0.941)
  the two profiles are of different devices: /device:TPU:16 before, /device:TPU:0 now
where the time goes in v1:
time: 239 us
  Pallas kernels  237 us (99%)
    pallas_call x1, Pallas kernels, on_device(): pl.pallas_call(functools.partial(kernel, n_grp, n_fs, n_tp, n_sub), out_s...  228 us
    pallas_call x1, Pallas kernels, on_device(): pl.pallas_call(functools.partial(store, parts), out_shape=[bf16((tokens,...  8.94 us

profile of v1, /device:TPU:0, one launch (start us, length us, event | category | flops | bytes accessed | tf_op | source)
XLA Modules:
  0.0 238.6 jit_solution(153088470653621888)
XLA Ops:
  0.6 0.0 copy-start
  0.6 0.7 copy-done
  1.3 0.0 copy-start.1
  1.3 0.7 copy-done.1
  2.0 227.6 %serve.1 = (bf16[8,256,256]{2,1,0:T(8,128)(2,1)S(1)}, bf16[2048,1024]{1,0:T(8,128)(2,1)S(1)}, bf16[2048,1024]{1,0:T(8,128)(2,1)S(1)}, bf16[2048,1024]{1,0:T(8,12...) custom-call(bf16[256,2048]{1,0:T(8,128)(2,1)} %refs_0_.1, ...), custom_call_target="tpu_custom_call" | custom-call | tf_op jit(solution)/shard_map/serve/pallas_call | solution.py:548
  229.6 8.9 %store.1 = (bf16[256,2048]{1,0:T(8,128)(2,1)}, bf16[2048,1024]{1,0:T(8,128)(2,1)}, bf16[2048,1024]{1,0:T(8,128)(2,1)}, bf16[2048,1024]{1,0:T(8,128)(2,1)}, bf16[...) custom-call(bf16[8,256,256]{2,1,0:T(8,128)(2,1)S(1)} %get-tuple-element.21.refs_0_, ...), custom_call_target="tpu_custom_call" | custom-call | tf_op jit(solution)/shard_map/store/pallas_call | solution.py:573
Async XLA Ops:
  0.6 0.7 copy-start
  1.3 0.7 copy-start.1

commit v2 on v1

--- a/solution.py
+++ b/solution.py
@@ -11,6 +11,10 @@
 MESH = pl.DeviceIdType.MESH
 LANES = 128
 LAG = 2
+HALVES = 2
+SPLIT = 4
+WHOLE = (False, False, True, False)
+DIRECT = (True, True)
 
 
 def kernel(n_grp, n_fs, n_tp, n_sub, *refs):
@@ -26,10 +30,15 @@
     ratio = n_fs // n_tp
     chips = n_tp // 2
     home = f // ratio
-    mine_sub = lax.rem(t + n_tp - home, n_tp) // 2
+    mine_sub = lax.rem(t // 2 + chips - home // 2, chips)
     carries = mine_sub < n_sub
-    is_lane = lax.rem(t, 2) == lax.rem(home, 2)
     partner = t + 1 - 2 * lax.rem(t, 2)
+
+    def lane(m):
+        return lax.rem(t + m, 2) == lax.rem(home, 2)
+
+    def other_lane(m):
+        return lax.rem(t + m, 2) != lax.rem(home, 2)
 
     half = n_fs // 2
     lower = f < half
@@ -38,8 +47,13 @@
     toward = jnp.where(lower, f + 1, f - 1)
     away = jnp.where(lower, jnp.maximum(f - 1, 0), jnp.minimum(f + 1, n_fs - 1))
 
+    step = jnp.where(lower, 1, n_fs - 1)
+
     def along_fs(o):
         return lax.rem(f + o, n_fs)
+
+    def by_way(o):
+        return lax.rem(f + o * step, n_fs)
 
     def along_tp(dx):
         return lax.rem(t + 2 * dx, n_tp)
@@ -58,7 +72,8 @@
 
     rows, columns = weights[0].shape
     share = rows // n_grp
-    sub = share // n_sub
+    subs = [1 if whole else n_sub for whole in WHOLE]
+    columns_to = [chips if whole else n_sub for whole in WHOLE]
     width = served[0].shape[1]
     d_rows, d_cols = downs[0].shape
     d_share = d_rows // n_grp
@@ -67,6 +82,7 @@
     tile = min(256, width)
     wide = min(256, features)
     chunks = features // wide
+    halves, part_rows, _ = result.shape[0] // chunks, *result.shape[1:]
 
     def landing(n):
         return land[n % 3] if n < 4 else land[3]
@@ -104,29 +120,42 @@
             to = pl.ds(pl.multiple_of(t * d_cols, d_cols), d_cols)
             served_down[k][at, to] = landing(4 + k)[at].astype(jnp.bfloat16)
 
+    def carried(m, s):
+        return 0 if WHOLE[m] else s
+
     def piece(m, r, h, s):
+        sub = share // subs[m]
         return served[m].at[pl.ds(pl.multiple_of(r * rows + h * share + s * sub, sub), sub)]
 
+    def own_rows(m, s):
+        sub = share // subs[m]
+        return pl.ds(pl.multiple_of(g * share + carried(m, s) * sub, sub), sub)
+
     def p_copy(m, s):
-        src = own.at[m, pl.ds(pl.multiple_of(g * share + s * sub, sub), sub)]
-        return remote(src, stage.at[m, s - 1], p_send.at[m, s - 1], p_recv.at[m, s - 1], {"tp": along_tp(s)})
+        src = own.at[m, own_rows(m, s)]
+        return remote(src, stage[m].at[s - 1], p_send.at[m, s - 1], p_recv.at[m, s - 1], {"tp": along_tp(s)})
 
     def p_start(m):
-        for s in range(1, n_sub):
+        for s in range(1, columns_to[m]):
             p_copy(m, s).start()
 
     def z_copy(m, s, j):
         cut = pl.ds(j * width, width)
         if s == 0:
-            src = own.at[m, pl.ds(pl.multiple_of(g * share, share), sub), cut]
-            return src, piece(m, f, g, s), t * ratio + j
+            return own.at[m, own_rows(m, 0), cut], piece(m, f, g, 0), t * ratio + j
         source = lax.rem(t + n_tp - 2 * s, n_tp)
-        return stage.at[m, s - 1, :, cut], piece(m, f, g, s), source * ratio + j
+        return stage[m].at[s - 1, :, cut], piece(m, f, g, carried(m, s)), source * ratio + j
 
     def z_remote(m, s, j):
         src, dst, to = z_copy(m, s, j)
         send = z_send.at[m, j] if s == 0 else r_send.at[m, s - 1, j]
-        return remote(src, dst, send, z_recv.at[m, f], {"fs": to})
+        where = {"fs": to} if m % 2 == 0 else {"fs": to, "tp": partner}
+        return remote(src, dst, send, z_recv.at[m, f], where)
+
+    def z_aside(m, s, j):
+        src, dst, _ = z_copy(m, s, j)
+        send = z_send.at[m, j] if s == 0 else r_send.at[m, s - 1, j]
+        return remote(src, dst, send, own_sem.at[m], {"tp": partner})
 
     def z_start(m, s):
         for j in range(ratio):
@@ -138,11 +167,14 @@
 
             @pl.when(to == f)
             def _():
-                pltpu.make_async_copy(src, dst, own_sem.at[m]).start()
+                if m % 2 == 0:
+                    pltpu.make_async_copy(src, dst, own_sem.at[m]).start()
+                else:
+                    z_aside(m, s, j).start()
 
     def relay(m):
-        for s in range(1, n_sub):
-            arrived(stage.at[m, s - 1], p_recv.at[m, s - 1])
+        for s in range(1, columns_to[m]):
+            arrived(stage[m].at[s - 1], p_recv.at[m, s - 1])
             z_start(m, s)
 
     def x_copy(m, r, dx):
@@ -157,32 +189,47 @@
         ref = piece(m, r, h, s)
         return remote(ref, ref, c_send.at[m, r, h, s], c_recv.at[m, r, h, s], {"tp": partner})
 
-    def primary(m):
-        @pl.when(is_lane)
-        def _():
-            @pl.loop(0, n_fs)
+    def primary_step(m, o):
+        r = by_way(o)
+        s = 0 if WHOLE[m] else mine_sub
+        ref = piece(m, r, g, s)
+
+        def onward_from(first):
+            arrived(ref, own_sem.at[m] if first else z_recv.at[m, r])
+            if not WHOLE[m]:
+                for dx in range(1, chips):
+                    x_copy(m, r, dx).start()
+            for dg in range(1, n_grp):
+                y_copy(m, r, dg, s).start()
+            c_copy(m, r, g, s).start()
+
+        if WHOLE[m]:
+            onward_from(isinstance(o, int))
+        else:
+            @pl.when(carries)
+            def _():
+                onward_from(isinstance(o, int))
+
+    def own_first(m):
+        @pl.when(jnp.logical_and(lane(m), mine_sub == 0))
+        def _():
+            primary_step(m, 0)
+
+    def own_later(m):
+        @pl.when(jnp.logical_and(lane(m), mine_sub != 0))
+        def _():
+            primary_step(m, 0)
+
+    def primary(m, low=1, high=n_fs):
+        @pl.when(lane(m))
+        def _():
+            @pl.loop(low, high)
             def _(o):
-                r = along_fs(o)
-
-                @pl.when(carries)
-                def _():
-                    @pl.when(o == 0)
-                    def _():
-                        arrived(piece(m, r, g, mine_sub), own_sem.at[m])
-
-                    @pl.when(o != 0)
-                    def _():
-                        arrived(piece(m, r, g, mine_sub), z_recv.at[m, r])
-
-                    for dx in range(1, chips):
-                        x_copy(m, r, dx).start()
-                    for dg in range(1, n_grp):
-                        y_copy(m, r, dg, mine_sub).start()
-                    c_copy(m, r, g, mine_sub).start()
+                primary_step(m, o)
 
     def crossed_step(m, o):
-        r = along_fs(o)
-        for s in range(n_sub):
+        r = by_way(o)
+        for s in range(0 if WHOLE[m] else n_sub):
             @pl.when(mine_sub != s)
             def _():
                 arrived(piece(m, r, g, s), x_recv.at[m, r, s])
@@ -191,34 +238,39 @@
                 c_copy(m, r, g, s).start()
 
     def crossed(m):
-        @pl.when(is_lane)
+        @pl.when(lane(m))
         def _():
             @pl.loop(0, n_fs)
             def _(o):
                 crossed_step(m, o)
 
+    def secondary_step(m, o):
+        r = by_way(o)
+        for dg in range(1, n_grp):
+            h = along_grp(dg)
+            for s in range(subs[m]):
+                arrived(piece(m, r, h, s), y_recv.at[m, r, h, s])
+                c_copy(m, r, h, s).start()
+
     def secondary(m):
-        @pl.when(is_lane)
+        @pl.when(lane(m))
         def _():
             @pl.loop(0, n_fs)
             def _(o):
-                r = along_fs(o)
-                for dg in range(1, n_grp):
-                    h = along_grp(dg)
-                    for s in range(n_sub):
-                        arrived(piece(m, r, h, s), y_recv.at[m, r, h, s])
-                        c_copy(m, r, h, s).start()
-
-    def complete(m):
-        @pl.when(jnp.logical_not(is_lane))
+                secondary_step(m, o)
+
+    def complete(m, groups):
+        @pl.when(other_lane(m))
         def _():
             @pl.loop(0, n_fs)
-            def _(r):
-                for h in range(n_grp):
-                    for s in range(n_sub):
-                        arrived(piece(m, r, h, s), c_recv.at[m, r, h, s])
-
-    direct = (True, False)
+            def _(o):
+                r = by_way(o)
+                for dg in groups:
+                    for s in range(subs[m]):
+                        arrived(piece(m, r, along_grp(dg), s), c_recv.at[m, r, along_grp(dg), s])
+
+    near, far = range(1), range(1, n_grp)
+    direct = DIRECT
 
     def d_piece(k, s, h):
         return served_down[k].at[
@@ -282,61 +334,78 @@
         ref = final[k].at[i]
         return remote(ref, ref, o_send.at[k, i], o_recv.at[k, i], {"fs": away})
 
+    def place(n):
+        i, h = n // halves, lax.rem(n, halves)
+        return (
+            pl.ds(pl.multiple_of(h * part_rows, part_rows), part_rows),
+            pl.ds(pl.multiple_of(i * wide, wide), wide),
+        )
+
     def gather_in(k, i):
         at = pl.ds(pl.multiple_of(i * wide, wide), wide)
         value = jnp.dot(hidden[...], served_down[k][:, at], preferred_element_type=jnp.float32)
-
-        @pl.when(is_end)
-        def _():
-            onward[k, i] = value.astype(jnp.bfloat16)
+        for h in range(halves):
+            n = i * halves + h
+            own_part = value[h * part_rows : (h + 1) * part_rows]
+
+            @pl.when(is_end)
+            def _():
+                onward[k, n] = own_part.astype(jnp.bfloat16)
+
+            @pl.when(jnp.logical_not(is_end))
+            def _():
+                arrived(inward.at[k, n], u_recv.at[k, n])
+                onward[k, n] = (own_part + inward[k, n].astype(jnp.float32)).astype(jnp.bfloat16)
+
+            @pl.when(is_mid)
+            def _():
+                to_middle(k, n).start()
+
+            @pl.when(jnp.logical_not(is_mid))
+            def _():
+                to_next(k, n).start()
+
+    def spread_out(k, n):
+        at = place(n)
+
+        @pl.when(is_mid)
+        def _():
+            arrived(middle.at[k, n], m_recv.at[k, n])
+            total = 0.5 * (onward[k, n].astype(jnp.float32) + middle[k, n].astype(jnp.float32))
+            if k == 1:
+                total = stream[at] + total
+            final[k][n] = total.astype(jnp.bfloat16)
+
+        @pl.when(jnp.logical_not(is_mid))
+        def _():
+            arrived(final[k].at[n], o_recv.at[k, n])
 
         @pl.when(jnp.logical_not(is_end))
         def _():
-            arrived(inward.at[k, i], u_recv.at[k, i])
-            onward[k, i] = (value + inward[k, i].astype(jnp.float32)).astype(jnp.bfloat16)
-
-        @pl.when(is_mid)
-        def _():
-            to_middle(k, i).start()
-
-        @pl.when(jnp.logical_not(is_mid))
-        def _():
-            to_next(k, i).start()
-
-    def spread_out(k, i):
-        at = pl.ds(pl.multiple_of(i * wide, wide), wide)
-
-        @pl.when(is_mid)
-        def _():
-            arrived(middle.at[k, i], m_recv.at[k, i])
-            total = 0.5 * (onward[k, i].astype(jnp.float32) + middle[k, i].astype(jnp.float32))
-            if k == 1:
-                total = stream[:, at] + total
-            final[k][i] = total.astype(jnp.bfloat16)
-
-        @pl.when(jnp.logical_not(is_mid))
-        def _():
-            arrived(final[k].at[i], o_recv.at[k, i])
-
-        @pl.when(jnp.logical_not(is_end))
-        def _():
-            to_outer(k, i).start()
+            to_outer(k, n).start()
 
         if k == 0:
-            stream[:, at] = stream[:, at] + delta[i].astype(jnp.float32)
+            stream[at] = stream[at] + delta[n].astype(jnp.float32)
 
     def reduce(k, beside=None):
-        @pl.loop(0, chunks + LAG)
+        lag = jnp.where(is_mid, LAG, chunks)
+        first = jnp.where(is_mid, 1, chunks)
+
+        @pl.loop(0, jnp.where(is_mid, chunks + LAG, 2 * chunks))
         def _(i):
             @pl.when(i < chunks)
             def _():
                 gather_in(k, i)
-                if beside is not None:
-                    beside(i)
-
-            @pl.when(i >= LAG)
-            def _():
-                spread_out(k, i - LAG)
+
+            if beside is not None:
+                @pl.when(i >= first)
+                def _():
+                    beside(i - first)
+
+            @pl.when(i >= lag)
+            def _():
+                for h in range(halves):
+                    spread_out(k, (i - lag) * halves + h)
 
     def norm():
         @pl.loop(0, tokens // slab)
@@ -364,6 +433,7 @@
     barrier = pltpu.get_barrier_semaphore()
     peers = (
         [{"fs": along_fs(o)} for o in range(1, n_fs)]
+        + [{"fs": along_fs(o), "tp": partner} for o in range(1, n_fs)]
         + [{"tp": along_tp(dx)} for dx in range(1, chips)]
         + [{"grp": along_grp(dg)} for dg in range(1, n_grp)]
         + [{"tp": partner}]
@@ -381,66 +451,73 @@
     p_start(1)
     z_start(1, 0)
     spread_gain(1)
+    fold(2)
+    p_start(2)
     round_down(0)
     load(5).start()
-    fold(2)
     fold(3)
     round_down(1)
     prompt_copy.wait()
     stream[...] = normed[...].astype(jnp.float32)
     norm()
 
+    own_first(0)
+    own_first(1)
     relay(0)
+    own_later(0)
+    primary(0, 1, 2)
     relay(1)
-    primary(0)
-    p_start(2)
+    own_later(1)
+    primary(0, 2)
+    primary(1)
     z_start(2, 0)
-    primary(1)
+    own_first(2)
+    relay(2)
+    own_later(2)
     p_start(3)
     z_start(3, 0)
+    own_first(3)
     crossed(0)
-    relay(2)
+    crossed(1)
     down_start(0)
-    crossed(1)
     relay(3)
+    own_later(3)
     primary(2)
-    primary(3)
-    down_secondary(0)
     secondary(0)
     secondary(1)
-    complete(0)
-    complete(1)
+    for m in (0, 1):
+        complete(m, near)
+        complete(m, far)
     multiply(0)
+    primary(3)
     down_start(1)
+    down_secondary(0)
 
     def beside(i):
-        @pl.when(is_lane)
-        def _():
-            per = -(-2 * n_fs // chunks)
-            for q in range(per):
-                n = i * per + q
-
-                @pl.when(n < n_fs)
-                def _():
-                    crossed_step(2, n)
-
-                @pl.when(jnp.logical_and(n >= n_fs, n < 2 * n_fs))
-                def _():
-                    crossed_step(3, n - n_fs)
+        per = -(-n_fs // chunks)
+        for q in range(per):
+            n = i * per + q
+
+            @pl.when(jnp.logical_and(lane(2), n < n_fs))
+            def _():
+                secondary_step(2, n)
+
+            @pl.when(jnp.logical_and(lane(3), n < n_fs))
+            def _():
+                crossed_step(3, n)
 
     reduce(0, beside)
     norm()
-    down_primary(1)
-    secondary(2)
     secondary(3)
-    complete(2)
-    complete(3)
+    for m in (2, 3):
+        complete(m, near)
+        complete(m, far)
     multiply(1)
     down_secondary(1)
     reduce(1)
 
     for m in range(4):
-        for s in range(n_sub):
+        for s in range(columns_to[m]):
             if s > 0:
                 p_copy(m, s).wait_send()
             for j in range(ratio):
@@ -448,16 +525,22 @@
                 def _():
                     z_remote(m, s, j).wait_send()
 
-        @pl.when(is_lane)
+                if m % 2 == 1:
+                    @pl.when(z_copy(m, s, j)[2] == f)
+                    def _():
+                        z_aside(m, s, j).wait_send()
+
+        @pl.when(lane(m))
         def _():
             @pl.loop(0, n_fs)
             def _(r):
-                @pl.when(carries)
-                def _():
-                    for dx in range(1, chips):
-                        x_copy(m, r, dx).wait_send()
-
-                for s in range(n_sub):
+                if not WHOLE[m]:
+                    @pl.when(carries)
+                    def _():
+                        for dx in range(1, chips):
+                            x_copy(m, r, dx).wait_send()
+
+                for s in range(subs[m]):
                     for dg in range(1, n_grp):
                         y_copy(m, r, dg, s).wait_send()
                     for h in range(n_grp):
@@ -472,7 +555,7 @@
                 for dg in range(1, n_grp):
                     dy_copy(k, dx, dg).wait_send()
 
-        @pl.loop(0, chunks)
+        @pl.loop(0, chunks * halves)
         def _(i):
             @pl.when(is_mid)
             def _():
@@ -487,12 +570,13 @@
                 to_outer(k, i).wait_send()
 
 
-def store(parts, *refs):
+def store(halves, parts, *refs):
     ins, outs, sems = refs[:7], refs[7:14], refs[14]
     copies = []
-    chunks, _, wide = ins[0].shape
-    for i in range(chunks):
-        copies.append((ins[0].at[i], outs[0].at[:, pl.ds(i * wide, wide)]))
+    pieces, rows, wide = ins[0].shape
+    for n in range(pieces):
+        at = pl.ds(n % halves * rows, rows), pl.ds(n // halves * wide, wide)
+        copies.append((ins[0].at[n], outs[0].at[at]))
     for src, dst in zip(ins[1:], outs[1:]):
         rows = src.shape[0] // parts
         for i in range(parts):
@@ -523,7 +607,9 @@
     d_rows, d_cols = down_first.shape
     chips = n_tp // 2
     wide = min(256, features)
+    halves = HALVES if tokens % (16 * HALVES) == 0 else 1
     chunks = features // wide
+    parts = (chunks * halves, tokens // halves, wide)
     gate_shape, down_shape = (features, width), (d_rows, features)
     bf16 = functools.partial(jax.ShapeDtypeStruct, dtype=jnp.bfloat16)
     share = rows // n_grp
@@ -536,7 +622,7 @@
         (4, n_fs, n_grp, n_sub), (4, n_fs, n_grp, n_sub), (4, n_fs, n_grp, n_sub), (4,),
         (2, other_x), (2, other_x), (2, other_x, other_g), (2, other_x, other_g),
         (2, chips), (2, chips),
-        (2, chunks), (2, chunks), (2, chunks), (2, chunks), (2, chunks),
+        *[(2, parts[0])] * 5,
     ]
     if rows % LANES == 0:
         gains = [gain.reshape(1, rows) for gain in (gain_first, gain_second)]
@@ -544,7 +630,7 @@
         gains = [jnp.broadcast_to(gain[:, None], (rows, LANES)) for gain in (gain_first, gain_second)]
     far = functools.partial(pltpu.with_memory_space_constraint, memory_space=pltpu.HBM)
     vmem, hbm = pl.BlockSpec(memory_space=pltpu.VMEM), pl.BlockSpec(memory_space=pltpu.HBM)
-    shapes = [(chunks, tokens, wide)] + [gate_shape] * 4 + [down_shape] * 2
+    shapes = [parts] + [gate_shape] * 4 + [down_shape] * 2
     held = pl.pallas_call(
         functools.partial(kernel, n_grp, n_fs, n_tp, n_sub),
         out_shape=[bf16(s) for s in shapes],
@@ -557,25 +643,27 @@
             pltpu.VMEM((tokens, features), jnp.float32),
             pltpu.VMEM((tokens, features), jnp.bfloat16),
             pltpu.VMEM((tokens, width), jnp.bfloat16),
-            pltpu.VMEM((2, chunks, tokens, wide), jnp.bfloat16),
-            pltpu.VMEM((2, chunks, tokens, wide), jnp.bfloat16),
-            pltpu.VMEM((2, chunks, tokens, wide), jnp.bfloat16),
-            pltpu.VMEM((chunks, tokens, wide), jnp.bfloat16),
-            pltpu.VMEM((4, other_x, share // n_sub, columns), jnp.bfloat16),
+            pltpu.VMEM((2, *parts), jnp.bfloat16),
+            pltpu.VMEM((2, *parts), jnp.bfloat16),
+            pltpu.VMEM((2, *parts), jnp.bfloat16),
+            pltpu.VMEM(parts, jnp.bfloat16),
+            [
+                pltpu.VMEM((other_x, share // (1 if whole else n_sub), columns), jnp.bfloat16)
+                for whole in WHOLE
+            ],
         ]
         + [pltpu.SemaphoreType.DMA(s) for s in sems],
         compiler_params=pltpu.CompilerParams(
-            collective_id=0, has_side_effects=True, vmem_limit_bytes=26 * 2**20
+            collective_id=0, has_side_effects=True, vmem_limit_bytes=27 * 2**20
         ),
         name="serve",
     )(far(prompt), *gains, *map(far, (gate_first, up_first, gate_second, up_second, down_first, down_second)))
-    parts = 4
     result, g1, u1, g2, u2, d1, d2 = pl.pallas_call(
-        functools.partial(store, parts),
+        functools.partial(store, halves, SPLIT),
         out_shape=[bf16((tokens, features))] + [bf16(s) for s in shapes[1:]],
         in_specs=[vmem] * 7,
         out_specs=[hbm] * 7,
-        scratch_shapes=[pltpu.SemaphoreType.DMA((chunks + 6 * parts,))],
+        scratch_shapes=[pltpu.SemaphoreType.DMA((parts[0] + 6 * SPLIT,))],
         compiler_params=pltpu.CompilerParams(vmem_limit_bytes=2**20),
         name="store",
     )(*held)

time: 239 us -> 186 us (0.78)
  Pallas kernels: 237 us -> 183 us
    pallas_call x1, Pallas kernels: 228 us -> 174 us  [on_device(): pl.pallas_call(functools.partial(kernel, n_grp, n_fs, n_tp, n_sub), out_s...]
where the time goes in v2:
time: 186 us; the launch traced here: 185 us
  Pallas kernels  183 us (98%)
    pallas_call x1, Pallas kernels, on_device(): pl.pallas_call(functools.partial(kernel, n_grp, n_fs, n_tp, n_sub), out_s...  174 us
    pallas_call x1, Pallas kernels, on_device(): pl.pallas_call(functools.partial(store, halves, SPLIT), out_shape=[bf16((...  9.01 us

profile of v2, /device:TPU:0, one launch (start us, length us, event | category | flops | bytes accessed | tf_op | source)
XLA Modules:
  0.0 185.0 jit_solution(10137455814561183597)
XLA Ops:
  0.6 0.0 copy-start
  0.6 0.7 copy-done
  1.3 0.0 copy-start.1
  1.3 0.7 copy-done.1
  2.0 174.0 %serve.1 = (bf16[16,128,256]{2,1,0:T(8,128)(2,1)S(1)}, bf16[2048,1024]{1,0:T(8,128)(2,1)S(1)}, bf16[2048,1024]{1,0:T(8,128)(2,1)S(1)}, bf16[2048,1024]{1,0:T(8,1...) custom-call(bf16[256,2048]{1,0:T(8,128)(2,1)} %refs_0_.1, ...), custom_call_target="tpu_custom_call" | custom-call | tf_op jit(solution)/shard_map/serve/pallas_call | solution.py:634
  176.0 9.0 %store.1 = (bf16[256,2048]{1,0:T(8,128)(2,1)}, bf16[2048,1024]{1,0:T(8,128)(2,1)}, bf16[2048,1024]{1,0:T(8,128)(2,1)}, bf16[2048,1024]{1,0:T(8,128)(2,1)}, bf16[...) custom-call(bf16[16,128,256]{2,1,0:T(8,128)(2,1)S(1)} %get-tuple-element.21.refs_0_, ...), custom_call_target="tpu_custom_call" | custom-call | tf_op jit(solution)/shard_map/store/pallas_call | solution.py:661
Async XLA Ops:
  0.6 0.7 copy-start
  1.3 0.7 copy-start.1

commit v3 on v2

--- a/solution.py
+++ b/solution.py
@@ -11,20 +11,20 @@
 MESH = pl.DeviceIdType.MESH
 LANES = 128
 LAG = 2
+LEAD = 3
 HALVES = 2
 SPLIT = 4
-WHOLE = (False, False, True, False)
-DIRECT = (True, True)
+WHOLE = (False, False, False, False)
 
 
 def kernel(n_grp, n_fs, n_tp, n_sub, *refs):
     prompt, gains, weights, downs = refs[0], refs[1:3], refs[3:7], refs[7:9]
     result, served, served_down = refs[9], refs[10:14], refs[14:16]
-    (land, own, scale, stream, normed, hidden, onward, inward, middle, delta, stage) = refs[16:27]
-    (load_sem, prompt_sem,
+    (land, gain_land, own, scale, stream, normed, hidden, onward, inward, middle, delta, stage) = refs[16:28]
+    (load_sem, gain_sem, prompt_sem,
      p_send, p_recv, r_send, z_send, z_recv, x_send, x_recv, y_send, y_recv, c_send, c_recv, own_sem,
-     dx_send, dx_recv, dy_send, dy_recv, dc_send, dc_recv,
-     s_send, u_recv, m_recv, o_send, o_recv) = refs[27:]
+     dx_send, dx_recv, dc_send, dc_recv,
+     s_send, u_recv, m_recv, o_send, o_recv) = refs[28:]
 
     g, f, t = lax.axis_index("grp"), lax.axis_index("fs"), lax.axis_index("tp")
     ratio = n_fs // n_tp
@@ -47,13 +47,14 @@
     toward = jnp.where(lower, f + 1, f - 1)
     away = jnp.where(lower, jnp.maximum(f - 1, 0), jnp.minimum(f + 1, n_fs - 1))
 
-    step = jnp.where(lower, 1, n_fs - 1)
+    depth = jnp.where(lower, f, n_fs - 1 - f)
 
     def along_fs(o):
         return lax.rem(f + o, n_fs)
 
     def by_way(o):
-        return lax.rem(f + o * step, n_fs)
+        r = jnp.where(o <= depth, depth - o, o)
+        return jnp.where(lower, r, n_fs - 1 - r)
 
     def along_tp(dx):
         return lax.rem(t + 2 * dx, n_tp)
@@ -76,12 +77,12 @@
     columns_to = [chips if whole else n_sub for whole in WHOLE]
     width = served[0].shape[1]
     d_rows, d_cols = downs[0].shape
-    d_share = d_rows // n_grp
     tokens, features = prompt.shape
     slab = min(64, tokens)
     tile = min(256, width)
     wide = min(256, features)
     chunks = features // wide
+    strips = d_cols // wide
     halves, part_rows, _ = result.shape[0] // chunks, *result.shape[1:]
 
     def landing(n):
@@ -91,8 +92,12 @@
         src = weights[n] if n < 4 else downs[n - 4]
         return pltpu.make_async_copy(src, landing(n), load_sem.at[n])
 
+    def gain_copy(k):
+        return pltpu.make_async_copy(gains[k], gain_land.at[k], gain_sem.at[k])
+
     def spread_gain(k):
-        gain = gains[k]
+        gain_copy(k).wait()
+        gain = gain_land.at[k]
         if gain.shape[0] == rows:
             scale[k] = gain[...]
         else:
@@ -220,8 +225,10 @@
         def _():
             primary_step(m, 0)
 
-    def primary(m, low=1, high=n_fs):
-        @pl.when(lane(m))
+    straight = mine_sub == 0
+
+    def primary(m, where=True, low=1, high=n_fs):
+        @pl.when(jnp.logical_and(lane(m), where))
         def _():
             @pl.loop(low, high)
             def _(o):
@@ -237,10 +244,10 @@
                     y_copy(m, r, dg, s).start()
                 c_copy(m, r, g, s).start()
 
-    def crossed(m):
+    def crossed(m, low=0, high=n_fs):
         @pl.when(lane(m))
         def _():
-            @pl.loop(0, n_fs)
+            @pl.loop(low, high)
             def _(o):
                 crossed_step(m, o)
 
@@ -270,57 +277,33 @@
                         arrived(piece(m, r, along_grp(dg), s), c_recv.at[m, r, along_grp(dg), s])
 
     near, far = range(1), range(1, n_grp)
-    direct = DIRECT
-
-    def d_piece(k, s, h):
-        return served_down[k].at[
-            pl.ds(pl.multiple_of(h * d_share, d_share), d_share),
-            pl.ds(pl.multiple_of(s * d_cols, d_cols), d_cols),
-        ]
-
-    def d_block(k, s):
-        return served_down[k].at[:, pl.ds(pl.multiple_of(s * d_cols, d_cols), d_cols)]
-
-    def d_first(k, s):
-        return d_block(k, s) if direct[k] else d_piece(k, s, g)
-
-    def dx_copy(k, dx):
-        ref = d_first(k, t)
-        return remote(ref, ref, dx_send.at[k, dx - 1], dx_recv.at[k, dx - 1], {"tp": along_tp(dx)})
-
-    def dy_copy(k, dx, dg):
-        ref = d_piece(k, lax.rem(t + n_tp - 2 * dx, n_tp), g)
-        return remote(ref, ref, dy_send.at[k, dx - 1, dg - 1], dy_recv.at[k, dx - 1, dg - 1], {"grp": along_grp(dg)})
-
-    def dc_copy(k, dx):
-        ref = d_block(k, lax.rem(t + n_tp - 2 * dx, n_tp))
-        return remote(ref, ref, dc_send.at[k, dx], dc_recv.at[k, dx], {"tp": partner})
+
+    def d_strip(k, s, j):
+        return served_down[k].at[:, pl.ds(pl.multiple_of(s * d_cols + j * wide, wide), wide)]
+
+    def d_from(device, dx):
+        return lax.rem(device + n_tp - 2 * dx, n_tp)
+
+    def dx_copy(k, dx, j):
+        ref = d_strip(k, t, j)
+        return remote(ref, ref, dx_send.at[k, dx - 1, j], dx_recv.at[k, dx - 1, j], {"tp": along_tp(dx)})
+
+    def dc_copy(k, dx, j):
+        ref = d_strip(k, d_from(t, dx), j)
+        return remote(ref, ref, dc_send.at[k, dx, j], dc_recv.at[k, dx, j], {"tp": partner})
 
     def down_start(k):
-        for dx in range(1, chips):
-            dx_copy(k, dx).start()
-        dc_copy(k, 0).start()
-
-    def down_primary(k):
-        if direct[k]:
-            return
-        for dx in range(1, chips):
-            source = lax.rem(t + n_tp - 2 * dx, n_tp)
-            arrived(d_piece(k, source, g), dx_recv.at[k, dx - 1])
-            for dg in range(1, n_grp):
-                dy_copy(k, dx, dg).start()
-
-    def down_secondary(k):
-        for dx in range(1, chips):
-            source = lax.rem(t + n_tp - 2 * dx, n_tp)
-            if direct[k]:
-                arrived(d_block(k, source), dx_recv.at[k, dx - 1])
-            else:
-                for dg in range(1, n_grp):
-                    arrived(d_piece(k, source, lax.rem(g + n_grp - dg, n_grp)), dy_recv.at[k, dx - 1, dg - 1])
-            dc_copy(k, dx).start()
-        for dx in range(chips):
-            arrived(d_block(k, lax.rem(partner + n_tp - 2 * dx, n_tp)), dc_recv.at[k, dx])
+        for j in range(strips):
+            for dx in range(1, chips):
+                dx_copy(k, dx, j).start()
+            dc_copy(k, 0, j).start()
+
+    def down_pass(k, dx, j):
+        arrived(d_strip(k, d_from(t, dx), j), dx_recv.at[k, dx - 1, j])
+        dc_copy(k, dx, j).start()
+
+    def down_ready(k, dx, j):
+        arrived(d_strip(k, d_from(partner, dx), j), dc_recv.at[k, dx, j])
 
     final = (delta, result)
 
@@ -387,25 +370,42 @@
         if k == 0:
             stream[at] = stream[at] + delta[n].astype(jnp.float32)
 
+    per_chip = chunks // chips
+
+    def chunk_of(i):
+        chip = lax.rem(t // 2 + chips - i // per_chip, chips)
+        j = lax.rem(i, per_chip)
+        return chip * per_chip + lax.rem(j, 2) * strips + j // 2
+
     def reduce(k, beside=None):
         lag = jnp.where(is_mid, LAG, chunks)
-        first = jnp.where(is_mid, 1, chunks)
+        first = jnp.where(is_end, LEAD, 1)
 
         @pl.loop(0, jnp.where(is_mid, chunks + LAG, 2 * chunks))
         def _(i):
-            @pl.when(i < chunks)
-            def _():
-                gather_in(k, i)
-
             if beside is not None:
                 @pl.when(i >= first)
                 def _():
                     beside(i - first)
 
+            @pl.when(i < chunks)
+            def _():
+                for dx in range(1, chips):
+                    for j in range(strips):
+                        @pl.when(i == dx * per_chip + 2 * j - 1)
+                        def _():
+                            down_pass(k, dx, j)
+
+                        @pl.when(i == dx * per_chip + 2 * j)
+                        def _():
+                            down_ready(k, dx, j)
+
+                gather_in(k, chunk_of(i))
+
             @pl.when(i >= lag)
             def _():
                 for h in range(halves):
-                    spread_out(k, (i - lag) * halves + h)
+                    spread_out(k, chunk_of(i - lag) * halves + h)
 
     def norm():
         @pl.loop(0, tokens // slab)
@@ -425,8 +425,10 @@
             up = jnp.dot(normed[...], w_up[:, at], preferred_element_type=jnp.float32)
             hidden[:, at] = (jax.nn.silu(gate) * up).astype(jnp.bfloat16)
 
+    gain_copy(0).start()
     for n in (0, 1, 2, 4):
         load(n).start()
+    gain_copy(1).start()
     prompt_copy = pltpu.make_async_copy(prompt, normed, prompt_sem)
     prompt_copy.start()
 
@@ -452,7 +454,6 @@
     z_start(1, 0)
     spread_gain(1)
     fold(2)
-    p_start(2)
     round_down(0)
     load(5).start()
     fold(3)
@@ -465,55 +466,70 @@
     own_first(1)
     relay(0)
     own_later(0)
-    primary(0, 1, 2)
     relay(1)
     own_later(1)
-    primary(0, 2)
-    primary(1)
+    primary(0, True, 1, 2)
+    primary(1, True, 1, 2)
+    crossed(0, 0, 1)
+    crossed(1, 0, 1)
+    primary(0, True, 2)
+    primary(1, True, 2)
+    p_start(2)
     z_start(2, 0)
-    own_first(2)
-    relay(2)
-    own_later(2)
+    crossed(0, 1)
+    crossed(1, 1)
     p_start(3)
     z_start(3, 0)
+    down_start(0)
+    complete(0, near)
+    complete(1, near)
+    relay(2)
+    own_first(2)
+    secondary(0)
+    relay(3)
+    own_later(2)
+    primary(2, straight)
+    secondary(1)
+    complete(0, far)
+    complete(1, far)
+    multiply(0)
     own_first(3)
-    crossed(0)
-    crossed(1)
-    down_start(0)
-    relay(3)
     own_later(3)
-    primary(2)
-    secondary(0)
-    secondary(1)
-    for m in (0, 1):
-        complete(m, near)
-        complete(m, far)
-    multiply(0)
-    primary(3)
-    down_start(1)
-    down_secondary(0)
+    primary(3, straight)
+    for j in range(strips):
+        down_ready(0, 0, j)
+
+    crooked = jnp.logical_not(straight)
 
     def beside(i):
-        per = -(-n_fs // chunks)
-        for q in range(per):
-            n = i * per + q
-
-            @pl.when(jnp.logical_and(lane(2), n < n_fs))
-            def _():
-                secondary_step(2, n)
-
-            @pl.when(jnp.logical_and(lane(3), n < n_fs))
-            def _():
-                crossed_step(3, n)
+        @pl.when(i == 0)
+        def _():
+            primary(2, crooked)
+            primary(3, crooked)
+
+        @pl.when(i == 3)
+        def _():
+            down_start(1)
+
+        per = -(-n_fs // 4)
+        for m in (2, 3):
+            for q in range(per):
+                n = i // 2 * per + q
+
+                @pl.when(jnp.logical_and(lane(m), jnp.logical_and(lax.rem(i, 2) == 1, n < n_fs)))
+                def _():
+                    crossed_step(m, n)
 
     reduce(0, beside)
     norm()
+    secondary(2)
     secondary(3)
     for m in (2, 3):
         complete(m, near)
         complete(m, far)
     multiply(1)
-    down_secondary(1)
+    for j in range(strips):
+        down_ready(1, 0, j)
     reduce(1)
 
     for m in range(4):
@@ -547,13 +563,11 @@
                         c_copy(m, r, h, s).wait_send()
 
     for k in range(2):
-        dc_copy(k, 0).wait_send()
-        for dx in range(1, chips):
-            dx_copy(k, dx).wait_send()
-            dc_copy(k, dx).wait_send()
-            if not direct[k]:
-                for dg in range(1, n_grp):
-                    dy_copy(k, dx, dg).wait_send()
+        for j in range(strips):
+            dc_copy(k, 0, j).wait_send()
+            for dx in range(1, chips):
+                dx_copy(k, dx, j).wait_send()
+                dc_copy(k, dx, j).wait_send()
 
         @pl.loop(0, chunks * halves)
         def _(i):
@@ -610,18 +624,18 @@
     halves = HALVES if tokens % (16 * HALVES) == 0 else 1
     chunks = features // wide
     parts = (chunks * halves, tokens // halves, wide)
+    strips = d_cols // wide
     gate_shape, down_shape = (features, width), (d_rows, features)
     bf16 = functools.partial(jax.ShapeDtypeStruct, dtype=jnp.bfloat16)
     share = rows // n_grp
     n_sub = chips if share % (16 * chips) == 0 else 1
     other_x, other_g = max(chips - 1, 1), max(n_grp - 1, 1)
     sems = [
-        (6,), (),
+        (6,), (2,), (),
         (4, other_x), (4, other_x), (4, other_x, n_fs // n_tp),
         (4, n_fs // n_tp), (4, n_fs), (4, n_fs, other_x), (4, n_fs, n_sub), (4, n_fs, other_g, n_sub),
         (4, n_fs, n_grp, n_sub), (4, n_fs, n_grp, n_sub), (4, n_fs, n_grp, n_sub), (4,),
-        (2, other_x), (2, other_x), (2, other_x, other_g), (2, other_x, other_g),
-        (2, chips), (2, chips),
+        (2, other_x, strips), (2, other_x, strips), (2, chips, strips), (2, chips, strips),
         *[(2, parts[0])] * 5,
     ]
     if rows % LANES == 0:
@@ -634,10 +648,11 @@
     held = pl.pallas_call(
         functools.partial(kernel, n_grp, n_fs, n_tp, n_sub),
         out_shape=[bf16(s) for s in shapes],
-        in_specs=[hbm] + [vmem] * 2 + [hbm] * 6,
+        in_specs=[hbm] * 9,
         out_specs=[vmem] * 7,
         scratch_shapes=[
             [pltpu.VMEM((rows, columns), jnp.float32)] * 3 + [pltpu.VMEM((d_rows, d_cols), jnp.float32)],
+            pltpu.VMEM((2, *gains[0].shape), jnp.float32),
             pltpu.VMEM((4, rows, columns), jnp.bfloat16),
             pltpu.VMEM((2, rows, LANES), jnp.float32),
             pltpu.VMEM((tokens, features), jnp.float32),
@@ -657,7 +672,7 @@
             collective_id=0, has_side_effects=True, vmem_limit_bytes=27 * 2**20
         ),
         name="serve",
-    )(far(prompt), *gains, *map(far, (gate_first, up_first, gate_second, up_second, down_first, down_second)))
+    )(far(prompt), *map(far, gains), *map(far, (gate_first, up_first, gate_second, up_second, down_first, down_second)))
     result, g1, u1, g2, u2, d1, d2 = pl.pallas_call(
         functools.partial(store, halves, SPLIT),
         out_shape=[bf16((tokens, features))] + [bf16(s) for s in shapes[1:]],

time: 186 us -> 167 us (0.90)
  Pallas kernels: 183 us -> 166 us
    pallas_call x1, Pallas kernels: 174 us -> 157 us  [on_device(): pl.pallas_call(functools.partial(kernel, n_grp, n_fs, n_tp, n_sub), out_s...]
where the time goes in v3:
time: 167 us
  Pallas kernels  166 us (99%)
    pallas_call x1, Pallas kernels, on_device(): pl.pallas_call(functools.partial(kernel, n_grp, n_fs, n_tp, n_sub), out_s...  157 us
    pallas_call x1, Pallas kernels, on_device(): pl.pallas_call(functools.partial(store, halves, SPLIT), out_shape=[bf16((...  9.01 us

profile of v3, /device:TPU:0, one launch (start us, length us, event | category | flops | bytes accessed | tf_op | source)
XLA Modules:
  0.0 166.5 jit_solution(2308198171939869316)
XLA Ops:
  0.6 156.9 %serve.1 = (bf16[16,128,256]{2,1,0:T(8,128)(2,1)S(1)}, bf16[2048,1024]{1,0:T(8,128)(2,1)S(1)}, bf16[2048,1024]{1,0:T(8,128)(2,1)S(1)}, bf16[2048,1024]{1,0:T(8,1...) custom-call(bf16[256,2048]{1,0:T(8,128)(2,1)} %refs_0_.1, ...), custom_call_target="tpu_custom_call" | custom-call | tf_op jit(solution)/shard_map/serve/pallas_call | solution.py:648
  157.5 9.0 %store.1 = (bf16[256,2048]{1,0:T(8,128)(2,1)}, bf16[2048,1024]{1,0:T(8,128)(2,1)}, bf16[2048,1024]{1,0:T(8,128)(2,1)}, bf16[2048,1024]{1,0:T(8,128)(2,1)}, bf16[...) custom-call(bf16[16,128,256]{2,1,0:T(8,128)(2,1)S(1)} %get-tuple-element.21.refs_0_, ...), custom_call_target="tpu_custom_call" | custom-call | tf_op jit(solution)/shard_map/store/pallas_call | solution.py:676

commit v4 on v3

--- a/solution.py
+++ b/solution.py
@@ -10,7 +10,7 @@
 EPS = 1e-06
 MESH = pl.DeviceIdType.MESH
 LANES = 128
-LAG = 2
+LAG = 1
 LEAD = 3
 HALVES = 2
 SPLIT = 4
@@ -20,11 +20,11 @@
 def kernel(n_grp, n_fs, n_tp, n_sub, *refs):
     prompt, gains, weights, downs = refs[0], refs[1:3], refs[3:7], refs[7:9]
     result, served, served_down = refs[9], refs[10:14], refs[14:16]
-    (land, gain_land, own, scale, stream, normed, hidden, onward, inward, middle, delta, stage) = refs[16:28]
+    (land, gain_land, own, scale, stream, normed, hidden, opened, onward, inward, middle, delta, stage) = refs[16:29]
     (load_sem, gain_sem, prompt_sem,
      p_send, p_recv, r_send, z_send, z_recv, x_send, x_recv, y_send, y_recv, c_send, c_recv, own_sem,
      dx_send, dx_recv, dc_send, dc_recv,
-     s_send, u_recv, m_recv, o_send, o_recv) = refs[28:]
+     s_send, u_recv, back, o_send) = refs[29:]
 
     g, f, t = lax.axis_index("grp"), lax.axis_index("fs"), lax.axis_index("tp")
     ratio = n_fs // n_tp
@@ -132,6 +132,9 @@
         sub = share // subs[m]
         return served[m].at[pl.ds(pl.multiple_of(r * rows + h * share + s * sub, sub), sub)]
 
+    def rows_of(m, count):
+        return served[m].at[pl.ds(0, count)]
+
     def own_rows(m, s):
         sub = share // subs[m]
         return pl.ds(pl.multiple_of(g * share + carried(m, s) * sub, sub), sub)
@@ -184,15 +187,15 @@
 
     def x_copy(m, r, dx):
         ref = piece(m, r, g, mine_sub)
-        return remote(ref, ref, x_send.at[m, r, dx - 1], x_recv.at[m, r, mine_sub], {"tp": along_tp(dx)})
+        return remote(ref, ref, x_send.at[m], x_recv.at[m, r, mine_sub], {"tp": along_tp(dx)})
 
     def y_copy(m, r, dg, s):
         ref = piece(m, r, g, s)
-        return remote(ref, ref, y_send.at[m, r, dg - 1, s], y_recv.at[m, r, g, s], {"grp": along_grp(dg)})
+        return remote(ref, ref, y_send.at[m], y_recv.at[m, r, dg - 1, s], {"grp": along_grp(dg)})
 
     def c_copy(m, r, h, s):
         ref = piece(m, r, h, s)
-        return remote(ref, ref, c_send.at[m, r, h, s], c_recv.at[m, r, h, s], {"tp": partner})
+        return remote(ref, ref, c_send.at[m], c_recv.at[m, h], {"tp": partner})
 
     def primary_step(m, o):
         r = by_way(o)
@@ -226,6 +229,7 @@
             primary_step(m, 0)
 
     straight = mine_sub == 0
+    crooked = mine_sub != 0
 
     def primary(m, where=True, low=1, high=n_fs):
         @pl.when(jnp.logical_and(lane(m), where))
@@ -256,11 +260,11 @@
         for dg in range(1, n_grp):
             h = along_grp(dg)
             for s in range(subs[m]):
-                arrived(piece(m, r, h, s), y_recv.at[m, r, h, s])
+                arrived(piece(m, r, h, s), y_recv.at[m, r, n_grp - dg - 1, s])
                 c_copy(m, r, h, s).start()
 
-    def secondary(m):
-        @pl.when(lane(m))
+    def secondary(m, where=True):
+        @pl.when(jnp.logical_and(lane(m), where))
         def _():
             @pl.loop(0, n_fs)
             def _(o):
@@ -269,12 +273,8 @@
     def complete(m, groups):
         @pl.when(other_lane(m))
         def _():
-            @pl.loop(0, n_fs)
-            def _(o):
-                r = by_way(o)
-                for dg in groups:
-                    for s in range(subs[m]):
-                        arrived(piece(m, r, along_grp(dg), s), c_recv.at[m, r, along_grp(dg), s])
+            for dg in groups:
+                arrived(rows_of(m, n_fs * share), c_recv.at[m, along_grp(dg)])
 
     near, far = range(1), range(1, n_grp)
 
@@ -308,14 +308,14 @@
     final = (delta, result)
 
     def to_middle(k, i):
-        return remote(onward.at[k, i], middle.at[k, i], s_send.at[k, i], m_recv.at[k, i], {"fs": toward})
+        return remote(onward.at[k, i], middle.at[k, i], s_send.at[k], back.at[k, i], {"fs": toward})
 
     def to_next(k, i):
-        return remote(onward.at[k, i], inward.at[k, i], s_send.at[k, i], u_recv.at[k, i], {"fs": toward})
+        return remote(onward.at[k, i], inward.at[k, i], s_send.at[k], u_recv.at[k, i], {"fs": toward})
 
     def to_outer(k, i):
         ref = final[k].at[i]
-        return remote(ref, ref, o_send.at[k, i], o_recv.at[k, i], {"fs": away})
+        return remote(ref, ref, o_send.at[k], back.at[k, i], {"fs": away})
 
     def place(n):
         i, h = n // halves, lax.rem(n, halves)
@@ -353,7 +353,7 @@
 
         @pl.when(is_mid)
         def _():
-            arrived(middle.at[k, n], m_recv.at[k, n])
+            arrived(middle.at[k, n], back.at[k, n])
             total = 0.5 * (onward[k, n].astype(jnp.float32) + middle[k, n].astype(jnp.float32))
             if k == 1:
                 total = stream[at] + total
@@ -361,7 +361,7 @@
 
         @pl.when(jnp.logical_not(is_mid))
         def _():
-            arrived(final[k].at[n], o_recv.at[k, n])
+            arrived(final[k].at[n], back.at[k, n])
 
         @pl.when(jnp.logical_not(is_end))
         def _():
@@ -415,15 +415,19 @@
             factor = lax.rsqrt(jnp.mean(value * value, axis=-1, keepdims=True) + EPS)
             normed[at] = (value * factor).astype(jnp.bfloat16)
 
-    def multiply(k):
-        w_gate, w_up = served[2 * k], served[2 * k + 1]
-
+    def gate_part(k):
         @pl.loop(0, width // tile)
         def _(i):
             at = pl.ds(pl.multiple_of(i * tile, tile), tile)
-            gate = jnp.dot(normed[...], w_gate[:, at], preferred_element_type=jnp.float32)
-            up = jnp.dot(normed[...], w_up[:, at], preferred_element_type=jnp.float32)
-            hidden[:, at] = (jax.nn.silu(gate) * up).astype(jnp.bfloat16)
+            gate = jnp.dot(normed[...], served[2 * k][:, at], preferred_element_type=jnp.float32)
+            opened[:, at] = jax.nn.silu(gate)
+
+    def up_part(k):
+        @pl.loop(0, width // tile)
+        def _(i):
+            at = pl.ds(pl.multiple_of(i * tile, tile), tile)
+            up = jnp.dot(normed[...], served[2 * k + 1][:, at], preferred_element_type=jnp.float32)
+            hidden[:, at] = (opened[:, at] * up).astype(jnp.bfloat16)
 
     gain_copy(0).start()
     for n in (0, 1, 2, 4):
@@ -468,46 +472,55 @@
     own_later(0)
     relay(1)
     own_later(1)
+
+    @pl.when(crooked)
+    def _():
+        p_start(2)
+
     primary(0, True, 1, 2)
     primary(1, True, 1, 2)
     crossed(0, 0, 1)
     crossed(1, 0, 1)
     primary(0, True, 2)
     primary(1, True, 2)
-    p_start(2)
+
+    @pl.when(straight)
+    def _():
+        p_start(2)
+
     z_start(2, 0)
     crossed(0, 1)
     crossed(1, 1)
     p_start(3)
     z_start(3, 0)
     down_start(0)
+    relay(2)
     complete(0, near)
     complete(1, near)
-    relay(2)
     own_first(2)
     secondary(0)
+    own_later(2)
     relay(3)
-    own_later(2)
+    own_first(3)
+    own_later(3)
     primary(2, straight)
     secondary(1)
+    primary(2, crooked, 1, 2)
     complete(0, far)
+    gate_part(0)
     complete(1, far)
-    multiply(0)
-    own_first(3)
-    own_later(3)
+    up_part(0)
     primary(3, straight)
     for j in range(strips):
         down_ready(0, 0, j)
 
-    crooked = jnp.logical_not(straight)
-
     def beside(i):
         @pl.when(i == 0)
         def _():
-            primary(2, crooked)
+            primary(2, crooked, 2)
             primary(3, crooked)
 
-        @pl.when(i == 3)
+        @pl.when(i == 6)
         def _():
             down_start(1)
 
@@ -520,14 +533,24 @@
                 def _():
                     crossed_step(m, n)
 
+        for q in range(per):
+            n = (i - 8) * per + q
+            ripe = jnp.logical_and(n >= 0, n < n_fs)
+
+            @pl.when(jnp.logical_and(lane(2), jnp.logical_and(jnp.logical_not(is_mid), ripe)))
+            def _():
+                secondary_step(2, n)
+
     reduce(0, beside)
     norm()
-    secondary(2)
+    secondary(2, is_mid)
     secondary(3)
-    for m in (2, 3):
-        complete(m, near)
-        complete(m, far)
-    multiply(1)
+    complete(2, near)
+    complete(2, far)
+    gate_part(1)
+    complete(3, near)
+    complete(3, far)
+    up_part(1)
     for j in range(strips):
         down_ready(1, 0, j)
     reduce(1)
@@ -548,19 +571,15 @@
 
         @pl.when(lane(m))
         def _():
-            @pl.loop(0, n_fs)
-            def _(r):
-                if not WHOLE[m]:
-                    @pl.when(carries)
-                    def _():
-                        for dx in range(1, chips):
-                            x_copy(m, r, dx).wait_send()
-
-                for s in range(subs[m]):
-                    for dg in range(1, n_grp):
-                        y_copy(m, r, dg, s).wait_send()
-                    for h in range(n_grp):
-                        c_copy(m, r, h, s).wait_send()
+            if not WHOLE[m]:
+                @pl.when(carries)
+                def _():
+                    for dx in range(1, chips):
+                        arrived(rows_of(m, n_fs * (share // n_sub)), x_send.at[m])
+
+            for dg in range(1, n_grp):
+                arrived(rows_of(m, n_fs * share), y_send.at[m])
+            arrived(served[m], c_send.at[m])
 
     for k in range(2):
         for j in range(strips):
@@ -569,19 +588,11 @@
                 dx_copy(k, dx, j).wait_send()
                 dc_copy(k, dx, j).wait_send()
 
-        @pl.loop(0, chunks * halves)
-        def _(i):
-            @pl.when(is_mid)
-            def _():
-                to_middle(k, i).wait_send()
-
-            @pl.when(jnp.logical_not(is_mid))
-            def _():
-                to_next(k, i).wait_send()
-
-            @pl.when(jnp.logical_not(is_end))
-            def _():
-                to_outer(k, i).wait_send()
+        arrived(onward.at[k], s_send.at[k])
+
+        @pl.when(jnp.logical_not(is_end))
+        def _():
+            arrived(final[k], o_send.at[k])
 
 
 def store(halves, parts, *refs):
@@ -633,10 +644,10 @@
     sems = [
         (6,), (2,), (),
         (4, other_x), (4, other_x), (4, other_x, n_fs // n_tp),
-        (4, n_fs // n_tp), (4, n_fs), (4, n_fs, other_x), (4, n_fs, n_sub), (4, n_fs, other_g, n_sub),
-        (4, n_fs, n_grp, n_sub), (4, n_fs, n_grp, n_sub), (4, n_fs, n_grp, n_sub), (4,),
+        (4, n_fs // n_tp), (4, n_fs), (4,), (4, n_fs, n_sub), (4,), (4, n_fs, other_g, n_sub),
+        (4,), (4, n_grp), (4,),
         (2, other_x, strips), (2, other_x, strips), (2, chips, strips), (2, chips, strips),
-        *[(2, parts[0])] * 5,
+        (2,), (2, parts[0]), (2, parts[0]), (2,),
     ]
     if rows % LANES == 0:
         gains = [gain.reshape(1, rows) for gain in (gain_first, gain_second)]
@@ -658,6 +669,7 @@
             pltpu.VMEM((tokens, features), jnp.float32),
             pltpu.VMEM((tokens, features), jnp.bfloat16),
             pltpu.VMEM((tokens, width), jnp.bfloat16),
+            pltpu.VMEM((tokens, width), jnp.float32),
             pltpu.VMEM((2, *parts), jnp.bfloat16),
             pltpu.VMEM((2, *parts), jnp.bfloat16),
             pltpu.VMEM((2, *parts), jnp.bfloat16),

time: 167 us -> 157 us (0.940)
  Pallas kernels: 166 us -> 157 us
    pallas_call x1, Pallas kernels: 157 us -> 148 us  [on_device(): pl.pallas_call(functools.partial(kernel, n_grp, n_fs, n_tp, n_sub), out_s...]
where the time goes in v4:
time: 157 us
  Pallas kernels  157 us (100%)
    pallas_call x1, Pallas kernels, on_device(): pl.pallas_call(functools.partial(kernel, n_grp, n_fs, n_tp, n_sub), out_s...  148 us
    pallas_call x1, Pallas kernels, on_device(): pl.pallas_call(functools.partial(store, halves, SPLIT), out_shape=[bf16((...  9.01 us

profile of v4, /device:TPU:0, one launch (start us, length us, event | category | flops | bytes accessed | tf_op | source)
XLA Modules:
  0.0 157.2 jit_solution(2509071333743618957)
XLA Ops:
  0.6 147.5 %serve.1 = (bf16[16,128,256]{2,1,0:T(8,128)(2,1)S(1)}, bf16[2048,1024]{1,0:T(8,128)(2,1)S(1)}, bf16[2048,1024]{1,0:T(8,128)(2,1)S(1)}, bf16[2048,1024]{1,0:T(8,1...) custom-call(bf16[256,2048]{1,0:T(8,128)(2,1)} %refs_0_.1, ...), custom_call_target="tpu_custom_call" | custom-call | tf_op jit(solution)/shard_map/serve/pallas_call | solution.py:659
  148.2 9.0 %store.1 = (bf16[256,2048]{1,0:T(8,128)(2,1)}, bf16[2048,1024]{1,0:T(8,128)(2,1)}, bf16[2048,1024]{1,0:T(8,128)(2,1)}, bf16[2048,1024]{1,0:T(8,128)(2,1)}, bf16[...) custom-call(bf16[16,128,256]{2,1,0:T(8,128)(2,1)S(1)} %get-tuple-element.21.refs_0_, ...), custom_call_target="tpu_custom_call" | custom-call | tf_op jit(solution)/shard_map/store/pallas_call | solution.py:688

commit v5 on v4

--- a/solution.py
+++ b/solution.py
@@ -79,7 +79,7 @@
     d_rows, d_cols = downs[0].shape
     tokens, features = prompt.shape
     slab = min(64, tokens)
-    tile = min(256, width)
+    tile = min(512, width)
     wide = min(256, features)
     chunks = features // wide
     strips = d_cols // wide
@@ -505,7 +505,7 @@
     own_later(3)
     primary(2, straight)
     secondary(1)
-    primary(2, crooked, 1, 2)
+    primary(2, crooked)
     complete(0, far)
     gate_part(0)
     complete(1, far)
@@ -517,7 +517,6 @@
     def beside(i):
         @pl.when(i == 0)
         def _():
-            primary(2, crooked, 2)
             primary(3, crooked)
 
         @pl.when(i == 6)

time: 157 us -> 157 us (level)
  no operation moved by 1% of the time
where the time goes in v5:
time: 157 us
  Pallas kernels  156 us (99%)
    pallas_call x1, Pallas kernels, on_device(): pl.pallas_call(functools.partial(kernel, n_grp, n_fs, n_tp, n_sub), out_s...  147 us
    pallas_call x1, Pallas kernels, on_device(): pl.pallas_call(functools.partial(store, halves, SPLIT), out_shape=[bf16((...  9.01 us

profile of v5, /device:TPU:0, one launch (start us, length us, event | category | flops | bytes accessed | tf_op | source)
XLA Modules:
  0.0 156.7 jit_solution(9210691852416885185)
XLA Ops:
  0.6 147.0 %serve.1 = (bf16[16,128,256]{2,1,0:T(8,128)(2,1)S(1)}, bf16[2048,1024]{1,0:T(8,128)(2,1)S(1)}, bf16[2048,1024]{1,0:T(8,128)(2,1)S(1)}, bf16[2048,1024]{1,0:T(8,1...) custom-call(bf16[256,2048]{1,0:T(8,128)(2,1)} %refs_0_.1, ...), custom_call_target="tpu_custom_call" | custom-call | tf_op jit(solution)/shard_map/serve/pallas_call | solution.py:658
  147.7 9.0 %store.1 = (bf16[256,2048]{1,0:T(8,128)(2,1)}, bf16[2048,1024]{1,0:T(8,128)(2,1)}, bf16[2048,1024]{1,0:T(8,128)(2,1)}, bf16[2048,1024]{1,0:T(8,128)(2,1)}, bf16[...) custom-call(bf16[16,128,256]{2,1,0:T(8,128)(2,1)S(1)} %get-tuple-element.21.refs_0_, ...), custom_call_target="tpu_custom_call" | custom-call | tf_op jit(solution)/shard_map/store/pallas_call | solution.py:687
